TPU v7x, 32 devices: a whole 2x2x4 slice. The times are simulated.
32 devices in a mesh: grp: 2 (over x), ep: 16 (over z, y, core).
Axes of the slice: x: 2, y: 2, z: 4, core: 2. Of those that a mesh axis runs over, the one named last changes fastest.
Arguments:
- queries: bfloat16 [32, 8, 128], P(('grp', 'ep')), parts along dimension 0, may hold values from -400 to 400
- fresh_token_key: bfloat16 [32, 2, 128], P(('grp', 'ep')), parts along dimension 0, may hold values from -6 to 6
- value_new: bfloat16 [32, 2, 128], P(('grp', 'ep')), parts along dimension 0, may hold values from -6 to 6
- forget_logit: float32 [32, 8], P(('grp', 'ep')), parts along dimension 0, may hold values from -8 to 8
- cache_keys: bfloat16 [32, 2, 4096, 128], P(('grp', 'ep')), parts along dimension 0, may hold values from -12 to 12
- cache_values: bfloat16 [32, 2, 4096, 128], P(('grp', 'ep')), parts along dimension 0, may hold values from -6 to 6
- cache_cumlog: float32 [32, 8, 4096], P(('grp', 'ep')), parts along dimension 0, may hold values from -572 to 0
- lengths: int32 [32], P(('grp', 'ep')), parts along dimension 0, may hold values from 1024 to 4096
- residual: bfloat16 [32, 2048], P('grp', 'ep'), parts along dimension 0, may hold values from -6 to 6
- out_weight: bfloat16 [1024, 2048], P(None, 'ep'), may hold values from -0.1875 to 0.1875
- norm_gain: float32 [2048], replicated, may hold values from 0.1 to 1.9
- expert_gate: bfloat16 [16, 704, 2048], P('ep'), may hold values from -0.125 to 0.125
- expert_up: bfloat16 [16, 704, 2048], P('ep'), may hold values from -0.125 to 0.125
- expert_down: bfloat16 [16, 704, 2048], P('ep'), may hold values from -0.21875 to 0.21875
- shared_gate: bfloat16 [1408, 2048], P('ep'), may hold values from -0.125 to 0.125
- shared_up: bfloat16 [1408, 2048], P('ep'), may hold values from -0.125 to 0.125
- shared_down: bfloat16 [1408, 2048], P(None, 'ep'), may hold values from -0.15625 to 0.15625
- routes: int32 [32, 6], P('grp'), parts along dimension 0, may hold values from 0 to 15, all different within a row; in each aligned block of 16 rows (0 to 15, 16 to 31, ...) at most 12 rows name the same one
- route_scores: float32 [32, 6], P('grp'), parts along dimension 0, may hold values from 0.05 to 1
Outputs:
- updated: bfloat16 [32, 2048], P('grp', 'ep'), parts along dimension 0
There are 2 independent parts, one for each index of `grp`. A program takes and returns all parts, laid end to end along the dimension named above; an argument that names none is the same for every part. Nothing has to cross between parts.
Inputs may be any that keep to these rules, and one draw needn't show every extreme that they name: `routes`: each row names 6 different experts; no expert is named by more than 12 rows of a part, a bound that some block reaches.
All inputs are finite; a program needn't handle non-finite values.
Results may differ from a plain program's by a relative error of at most 0.0068.
Values may be sent and summed in bfloat16 or wider, within the bound.
No kernel may reach another device: no remote copies, remote signals or barrier semaphores. Data moves between devices by JAX's collectives and lax.ppermute only.
A program may use at most 64 MiB of HBM per device.

v0:
```python
import jax
import jax.numpy as jnp
from jax import lax
from jax.sharding import PartitionSpec as P

CAP = 12


norm_eps = 1e-06
routed_scale = 2.5
contract_last = (((1,), (1,)), ((), ()))


def expert_hidden(row_block, gate_matrix, up_matrix):
    gate_part = lax.dot_general(
        row_block, gate_matrix, contract_last, preferred_element_type=jnp.float32
    )
    up_part = lax.dot_general(
        row_block, up_matrix, contract_last, preferred_element_type=jnp.float32
    )
    return (jax.nn.silu(gate_part) * up_part).astype(jnp.bfloat16)


def attention(
    queries,
    fresh_token_key,
    value_new,
    forget_logit,
    cache_keys,
    cache_values,
    cache_cumlog,
    lengths,
):
    batch_rows, head_count, head_size = queries.shape
    key_heads = cache_keys.shape[1]
    cache_span = cache_keys.shape[2]
    groups = head_count // key_heads
    inv_root = head_size ** (-0.5)
    grouped_heads = queries.reshape(batch_rows, key_heads, groups, head_size)
    scores = (
        jnp.einsum(
            "bkgd,bkpd->bkgp", grouped_heads, cache_keys, preferred_element_type=jnp.float32
        ).reshape(batch_rows, head_count, cache_span)
        * inv_root
    )
    positions = lax.broadcasted_iota(jnp.int32, (1, 1, cache_span), 2)
    last_pos = (lengths - 1)[:, None, None]
    latest = jnp.sum(jnp.where(positions == last_pos, cache_cumlog, 0.0), axis=2)
    log_gate = jax.nn.log_sigmoid(forget_logit)
    scores = scores + (latest + log_gate)[:, :, None] - cache_cumlog
    visible = positions < lengths[:, None, None]
    scores = jnp.where(visible, scores, -jnp.inf)
    own_score = (
        jnp.einsum(
            "tiuh,tih->tiu", grouped_heads, fresh_token_key, preferred_element_type=jnp.float32
        ).reshape(batch_rows, head_count)
        * inv_root
    )
    top_score = jnp.maximum(jnp.max(scores, axis=2), own_score)
    weights = jnp.where(visible, jnp.exp(scores - top_score[:, :, None]), 0.0)
    own_weight = jnp.exp(own_score - top_score)
    denominator = jnp.sum(weights, axis=2) + own_weight
    weighted = jnp.einsum(
        "bkgp,bkpd->bkgd",
        weights.astype(jnp.bfloat16).reshape(batch_rows, key_heads, groups, cache_span),
        cache_values,
        preferred_element_type=jnp.float32,
    )
    own_rounded = lax.optimization_barrier(own_weight.astype(jnp.bfloat16)).astype(jnp.float32)
    own_value = jnp.repeat(value_new, groups, axis=1).astype(jnp.float32)
    numerator = (
        weighted.reshape(batch_rows, head_count, head_size) + own_rounded[:, :, None] * own_value
    )
    return (
        (numerator / denominator[:, :, None])
        .astype(jnp.bfloat16)
        .reshape(batch_rows, head_count * head_size)
    )


def on_device(
    queries,
    fresh_token_key,
    value_new,
    forget_logit,
    cache_keys,
    cache_values,
    cache_cumlog,
    lengths,
    residual,
    out_weight,
    norm_gain,
    expert_gate,
    expert_up,
    expert_down,
    shared_gate,
    shared_up,
    shared_down,
    routes,
    route_scores,
):
    attended = attention(
        queries,
        fresh_token_key,
        value_new,
        forget_logit,
        cache_keys,
        cache_values,
        cache_cumlog,
        lengths,
    )
    mixed = jnp.dot(
        lax.all_gather(attended, "ep", axis=0, tiled=True),
        out_weight,
        preferred_element_type=jnp.float32,
    )
    stream = (residual.astype(jnp.float32) + mixed).astype(jnp.bfloat16)
    full_rows = lax.all_gather(stream, "ep", axis=1, tiled=True)
    rows_wide = full_rows.astype(jnp.float32)
    inv_rms = lax.rsqrt(jnp.mean(rows_wide * rows_wide, axis=1, keepdims=True) + norm_eps)
    normed = (rows_wide * inv_rms * norm_gain).astype(jnp.bfloat16)
    gate_weights = route_scores / jnp.sum(route_scores, axis=1, keepdims=True) * routed_scale
    shared_mid = expert_hidden(normed, shared_gate, shared_up)
    my_expert = lax.axis_index("ep")
    expert_hits = routes == my_expert
    is_member = jnp.sum(expert_hits.astype(jnp.int32), axis=1)
    slot_rank = jnp.cumsum(is_member) - 1
    slot_ids = lax.broadcasted_iota(jnp.int32, (CAP, 1), 0)
    selector = (is_member[None, :] == 1) & (slot_rank[None, :] == slot_ids)
    picked = jnp.dot(
        selector.astype(jnp.bfloat16), normed, preferred_element_type=jnp.float32
    ).astype(jnp.bfloat16)
    hidden = expert_hidden(picked, expert_gate[0], expert_up[0])
    expert_out = jnp.dot(hidden, expert_down[0], preferred_element_type=jnp.float32).astype(
        jnp.bfloat16
    )
    received = lax.all_to_all(expert_out[None], "ep", split_axis=2, concat_axis=0, tiled=True)
    expert_count = received.shape[0]
    expert_ids = lax.broadcasted_iota(jnp.int32, (1, 1, expert_count), 2)
    all_hits = routes[:, :, None] == expert_ids
    membership = jnp.sum(all_hits.astype(jnp.int32), axis=1)
    share_all = jnp.sum(jnp.where(all_hits, gate_weights[:, :, None], 0.0), axis=1)
    rank_all = jnp.cumsum(membership, axis=0) - 1
    slot_grid = lax.broadcasted_iota(jnp.int32, (1, 1, CAP), 2)
    slot_mask = (membership[:, :, None] == 1) & (rank_all[:, :, None] == slot_grid)
    combiner = jnp.where(slot_mask, share_all[:, :, None], 0.0).reshape(
        routes.shape[0], expert_count * CAP
    )
    flat_slots = received.reshape(expert_count * CAP, received.shape[2]).astype(jnp.float32)
    routed_part = jnp.dot(combiner, flat_slots, precision=lax.Precision.HIGHEST)
    shared_part = jnp.dot(
        lax.all_gather(shared_mid, "ep", axis=1, tiled=True),
        shared_down,
        preferred_element_type=jnp.float32,
    )
    return (stream.astype(jnp.float32) + routed_part + shared_part).astype(jnp.bfloat16)


def solution(mesh):
    placed = (
        P(("grp", "ep"), None, None),
        P(("grp", "ep"), None, None),
        P(("grp", "ep"), None, None),
        P(("grp", "ep"), None),
        P(("grp", "ep"), None, None, None),
        P(("grp", "ep"), None, None, None),
        P(("grp", "ep"), None, None),
        P(("grp", "ep")),
        P("grp", "ep"),
        P(None, "ep"),
        P(),
        P("ep", None, None),
        P("ep", None, None),
        P("ep", None, None),
        P("ep", None),
        P("ep", None),
        P(None, "ep"),
        P("grp", None),
        P("grp", None),
    )
    return jax.shard_map(
        on_device, mesh=mesh, in_specs=placed, out_specs=P("grp", "ep"), check_vma=False
    )
```

profile of v0, /device:TPU:0, one launch (start us, length us, event | category | flops | bytes accessed | tf_op | source)
XLA Modules:
  0.0 110.7 jit_solution(4193211708962261572)
XLA Ops:
  0.0 0.0 copy-start
  0.0 0.9 fusion.47
  1.0 0.1 mul.105
  1.0 0.1 mul.106
  1.8 0.7 convert_reduce_fusion.1
  2.5 0.7 bitcast_convert_fusion
  3.2 0.1 copy.41
  3.3 0.1 add_reduce_fusion
  3.4 2.3 %convolution_multiply_fusion = f32[2,4,4096]{2,1,0:T(4,128)S(1)} fusion(bf16[2,4,128]{2,1,0:T(4,128)(2,1)} %bitcast.100, bf16[1,2,4096,128]{3,2,1,0:T(8,128)(2,1)} %param.23), kind=kOutput, calls=%fused_computation | convolution fusion | flops 8421376 | bytes 2230272 | tf_op jit(solution)/shard_map/bkgd,bkpd->bkgp/dot_general | solution.py:41
  5.7 0.1 mul.103
  5.7 1.1 select_reduce_fusion
  6.8 0.7 fusion.52
  7.5 1.1 %fusion.59 = (f32[8]{0:T(128)S(1)}, f32[1,8,4096]{2,1,0:T(8,128)S(1)}) fusion(f32[1,8,4096]{2,1,0:T(8,128)} %param.25, f32[1,8,4096]{2,1,0:T(8,128)S(1)} %mul.103, f32[8]{0:T(128)S(1)} %fusion.52, pred[4096]{0:T(1024)(128)(4,1)S(1)} %iota_compare_fusion.3), kind=kLoop, calls=%fused_computation.78 | loop fusion | flops 131064 | bytes 397376 | tf_op jit(solution)/shard_map/reduce_max | solution.py:59
  8.6 0.2 fusion.34
  8.9 2.0 %fusion.12 = f32[2,4,128]{2,1,0:T(4,128)S(1)} fusion(bf16[2,4,4096]{2,1,0:T(4,128)(2,1)S(1)} %reshape.347, bf16[1,2,4096,128]{3,2,1,0:T(8,128)(2,1)} %param.24), kind=kOutput, calls=%fused_computation.10 | convolution fusion | flops 8388608 | bytes 2166784 | tf_op jit(solution)/shard_map/bkgp,bkpd->bkgd/dot_general | solution.py:63
  10.9 0.1 mul.107
  10.9 0.1 div.38
  11.1 23.3 %all-gather = bf16[16,1,1024]{2,1,0:T(2,128)(2,1)S(1)} all-gather(bf16[1,1,1024]{2,1,0:T(2,128)(2,1)S(1)} %convert_bitcast_fusion), channel_id=1, replica_groups=mesh['grp'=2,'ep'=16] {'ep'}, dimensions={0}, use_global_device_ids=true | all-gather | bytes 34816 | tf_op jit(solution)/shard_map/all_gather | solution.py:113
  34.4 0.0 copy-done.1
  34.4 0.0 copy-done.5
  34.4 0.2 fusion.22
  34.5 17.6 %all_gather.10 = bf16[16,2048]{1,0:T(8,128)(2,1)S(1)} all-gather(bf16[16,128]{1,0:T(8,128)(2,1)S(1)} %fusion.22), channel_id=1, replica_groups=mesh['grp'=2,'ep'=16] {'ep'}, dimensions={1}, use_global_device_ids=true | all-gather | bytes 69632 | tf_op jit(solution)/shard_map/all_gather | solution.py:118
  52.1 0.1 fusion.28
  52.2 0.0 copy-done.2
  52.2 0.2 convolution_convert_fusion
  52.5 2.7 %fusion.4 = f32[12,704]{1,0:T(8,128)S(1)} fusion(bf16[12,2048]{1,0:T(8,128)(2,1)S(1)} %convolution_convert_fusion, bf16[1,704,2048]{2,1,0:T(8,128)(2,1)} %param.30), kind=kOutput, calls=%fused_computation.5 | convolution fusion | flops 34603008 | bytes 2966528 | tf_op jit(solution)/shard_map/dot_general | solution.py:15
  55.1 0.0 copy-done
  55.1 3.5 %fusion.9 = bf16[1,12,2048]{2,1,0:T(8,128)(2,1)S(1)} fusion(bf16[1,704,2048]{2,1,0:T(8,128)(2,1)S(1)} %copy-done, bf16[12,2048]{1,0:T(8,128)(2,1)S(1)} %convolution_convert_fusion, bf16[1,704,2048]{2,1,0:T(8,128)(2,1)} %param.31, f32[12,704]{1,0:T(8,128)S(1)} %fusion.4), kind=kOutput, calls=%fused_computation.9 | convolution fusion | flops 69281280 | bytes 5899264 | tf_op jit(solution)/shard_map/dot_general | solution.py:134
  58.6 2.0 %copy.42 = bf16[1,12,2048]{1,0,2:T(2,128)(2,1)} copy(bf16[1,12,2048]{2,1,0:T(8,128)(2,1)S(1)} %fusion.9) | data formatting | bytes 98304 | tf_op jit(solution)/shard_map/broadcast_in_dim | solution.py:137
  60.7 0.5 broadcast.203
  61.2 12.6 %reduce.5 = bf16[2048,12]{1,0:T(8,128)(2,1)S(1)} reduce(bf16[2048,1,12]{2,1,0:T(2,128)(2,1)} %bitcast.91, bf16[]{:T(256)} %broadcast.203), dimensions={1}, to_apply=%bitcast.76.reduce_sub_computation | reduce | bytes 98306
  73.8 1.6 %reshape.361 = bf16[16,2,768]{2,1,0:T(2,128)(2,1)} reshape(bf16[2048,12]{1,0:T(8,128)(2,1)S(1)} %reduce.5) | data formatting | bytes 98304
  75.3 3.5 %all-to-all-start = ((bf16[16,2,768]{2,1,0:T(2,128)(2,1)}), bf16[16,2,768]{2,1,0:T(2,128)(2,1)S(1)}, u32[]{:S(2)}, u32[]{:S(2)}) async-start(bf16[16,2,768]{2,1,0:T(2,128)(2,1)} %reshape.361), calls=%async_computation | async-start | bytes 98304 | tf_op jit(solution)/shard_map/all_to_all | solution.py:137
  78.8 0.0 copy-done.3
  78.8 0.1 convert_reduce_fusion
  79.0 0.0 copy-done.4
  79.0 0.1 select_reduce_fusion.1
  79.1 1.2 %fusion.56 = f32[16,88]{1,0:T(8,128)S(1)} fusion(bf16[88,2048]{1,0:T(8,128)(2,1)} %param.33, bf16[16,2048]{1,0:T(8,128)(2,1)S(1)} %all_gather.10, f32[2048]{0:T(1024)S(1)} %copy-done.2, f32[16]{0:T(128)S(1)} %add_rsqrt_fusion), kind=kOutput, calls=%fused_computation.77 | convolution fusion | flops 5898240 | bytes 439872 | tf_op jit(solution)/shard_map/dot_general | solution.py:15
  80.3 1.2 %fusion.25 = bf16[1,88,16]{1,2,0:T(8,128)(2,1)S(1)} fusion(bf16[88,2048]{1,0:T(8,128)(2,1)} %param.34, f32[16,88]{1,0:T(8,128)S(1)} %fusion.56, bf16[16,2048]{1,0:T(8,128)(2,1)S(1)} %all_gather.10, f32[2048]{0:T(1024)S(1)} %copy-done.2, f32[16]{0:T(128)S(1)} %add_rsqrt_fusion), kind=kOutput, calls=%fused_computation.22 | convolution fusion | flops 5906688 | bytes 442688 | tf_op jit(solution)/shard_map/dot_general | solution.py:18
  81.6 21.8 %all-gather.1 = bf16[16,88,16]{1,2,0:T(8,128)(2,1)S(1)} all-gather(bf16[1,88,16]{1,2,0:T(8,128)(2,1)S(1)} %fusion.25), channel_id=1, replica_groups=mesh['grp'=2,'ep'=16] {'ep'}, dimensions={0}, use_global_device_ids=true | all-gather | bytes 47872 | tf_op jit(solution)/shard_map/all_gather | solution.py:152
  103.4 0.1 reshape.357
  103.6 1.1 %fusion.60 = f32[16,128]{1,0:T(8,128)S(1)} fusion(bf16[1408,16]{0,1:T(8,128)(2,1)S(1)} %reshape.357, bf16[1408,128]{1,0:T(8,128)(2,1)} %param.35), kind=kOutput, calls=%fused_computation.79 | convolution fusion | flops 5767168 | bytes 413696 | tf_op jit(solution)/shard_map/dot_general | solution.py:151
  104.7 0.2 fusion.32
  104.9 0.1 select_n.39
  105.0 0.0 all-to-all-done
  105.0 2.5 %reshape.362 = bf16[2048,1,12]{2,1,0:T(2,128)(2,1)} reshape(bf16[16,2,768]{2,1,0:T(2,128)(2,1)S(1)} %all-to-all-done) | data formatting | bytes 98304
  107.5 2.3 %copy.43 = bf16[1,12,2048]{2,1,0:T(8,128)(2,1)S(1)} copy(bf16[1,12,2048]{1,0,2:T(2,128)(2,1)} %bitcast.92) | data formatting | bytes 98304 | tf_op jit(solution)/shard_map/all_to_all | solution.py:137
  109.9 0.8 fusion.23
  (28 shorter events, 0.3 us)
Async XLA Ops:
  0.0 55.1 %copy-start = (bf16[1,704,2048]{2,1,0:T(8,128)(2,1)S(1)}, bf16[1,704,2048]{2,1,0:T(8,128)(2,1)}, u32[]{:S(2)}) copy-start(bf16[1,704,2048]{2,1,0:T(8,128)(2,1)} %param.32) | copy-start | bytes 8650756
  0.0 34.4 %copy-start.1 = (bf16[1024,128]{1,0:T(8,128)(2,1)S(1)}, bf16[1024,128]{1,0:T(8,128)(2,1)}, u32[]{:S(2)}) copy-start(bf16[1024,128]{1,0:T(8,128)(2,1)} %param.28) | copy-start | bytes 786436
  0.0 34.4 %copy-start.5 = (bf16[16,128]{1,0:T(8,128)(2,1)S(1)}, bf16[16,128]{1,0:T(8,128)(2,1)}, u32[]{:S(2)}) copy-start(bf16[16,128]{1,0:T(8,128)(2,1)} %param.27) | copy-start | bytes 12292
  3.4 48.8 %copy-start.2 = (f32[2048]{0:T(1024)S(1)}, f32[2048]{0:T(1024)}, u32[]{:S(2)}) copy-start(f32[2048]{0:T(1024)} %param.29) | copy-start | bytes 24580
  58.6 20.2 %copy-start.3 = (s32[16,6]{0,1:T(8,128)S(1)}, s32[16,6]{0,1:T(8,128)}, u32[]{:S(2)}) copy-start(s32[16,6]{0,1:T(8,128)} %param.36) | copy-start | bytes 1156
  58.6 20.3 %copy-start.4 = (f32[16,6]{0,1:T(8,128)S(1)}, f32[16,6]{0,1:T(8,128)}, u32[]{:S(2)}) copy-start(f32[16,6]{0,1:T(8,128)} %param.37) | copy-start | bytes 1156
  75.3 29.7 %all-to-all-start = ((bf16[16,2,768]{2,1,0:T(2,128)(2,1)}), bf16[16,2,768]{2,1,0:T(2,128)(2,1)S(1)}, u32[]{:S(2)}, u32[]{:S(2)}) async-start(bf16[16,2,768]{2,1,0:T(2,128)(2,1)} %reshape.361), calls=%async_computation | async-start | bytes 98304 | tf_op jit(solution)/shard_map/all_to_all | solution.py:137
where the time goes:
time: 111 us
  blocking collectives  62.7 us (56%)
  other arithmetic  17.8 us (16%)
  matrix products  16.1 us (15%)
  local copies, waits for them, and re-layouts  9.72 us (9%)
  starting transfers between devices  3.5 us (3%)
    all_gather x1, blocking collectives, on_device(): lax.all_gather(attended, 'ep', axis=0, tiled=True)  23.3 us
    all_gather x1, blocking collectives, on_device(): lax.all_gather(shared_mid, 'ep', axis=1, tiled=True)  21.8 us
    all_gather x1, blocking collectives, on_device(): full_rows = lax.all_gather(stream, 'ep', axis=1, tiled=True)  17.6 us
    unnamed x2, other arithmetic  12.6 us
    unnamed x17, local copies, waits for them, and re-layouts  4.7 us
    dot_general x2, matrix products, expert_hidden(): lax.dot_general(row_block, gate_matrix, contract_last, preferred_element_...  3.89 us
    all_to_all x1, starting transfers between devices, on_device(): lax.all_to_all(expert_out[None], 'ep', split_axis=2, concat_axis=0, tiled...  3.5 us
    dot_general x1, matrix products, on_device(): jnp.dot(hidden, expert_down[0], preferred_element_type=jnp.float32)  3.49 us
  transfers between devices with their start and end apart: 1, of which 0 were waited for; matrix products, arithmetic and copies ran while one was open for 4% of the time, Pallas kernels for 0%

commit v1 on v0

--- a/solution.py
+++ b/solution.py
@@ -1,6 +1,8 @@
 import jax
 import jax.numpy as jnp
 from jax import lax
+from jax.experimental import pallas as pl
+from jax.experimental.pallas import tpu as pltpu
 from jax.sharding import PartitionSpec as P
 
 CAP = 12
@@ -78,7 +80,7 @@
     )
 
 
-def on_device(
+def plain_device(
     queries,
     fresh_token_key,
     value_new,
@@ -156,6 +158,324 @@
     return (stream.astype(jnp.float32) + routed_part + shared_part).astype(jnp.bfloat16)
 
 
+VMEM = pltpu.VMEM
+chunk_count = 4
+
+
+def in_vmem():
+    return pl.BlockSpec(memory_space=VMEM)
+
+
+def params(mib):
+    return pltpu.CompilerParams(vmem_limit_bytes=mib * 1024 * 1024)
+
+
+def attention_kernel(
+    lengths_ref,
+    queries_ref,
+    fresh_ref,
+    value_new_ref,
+    forget_ref,
+    keys_hbm,
+    values_hbm,
+    cumlog_hbm,
+    out_ref,
+    keys,
+    values,
+    cumlog,
+    sems,
+):
+    heads, size = queries_ref.shape
+    key_heads, span, _ = keys.shape
+    groups = heads // key_heads
+    step = span // chunk_count
+    inv_root = size ** (-0.5)
+    cumlog_copy = pltpu.make_async_copy(cumlog_hbm.at[0], cumlog, sems.at[2 * chunk_count])
+    cumlog_copy.start()
+
+    def copies(source, target, first):
+        return [
+            pltpu.make_async_copy(
+                source.at[0, :, pl.ds(c * step, step), :],
+                target.at[:, pl.ds(c * step, step), :],
+                sems.at[first + c],
+            )
+            for c in range(chunk_count)
+        ]
+
+    key_copies = copies(keys_hbm, keys, 0)
+    value_copies = copies(values_hbm, values, chunk_count)
+    for copy in key_copies + value_copies:
+        copy.start()
+
+    length = lengths_ref[0]
+    queries = queries_ref[...]
+    head_rows = lax.broadcasted_iota(jnp.int32, (heads, 1), 0)
+    wide = jnp.concatenate(
+        [jnp.where(head_rows // groups == k, queries, jnp.zeros_like(queries)) for k in range(key_heads)],
+        axis=1,
+    )
+
+    def per_head(ref):
+        rows = ref[...].astype(jnp.float32)
+        total = jnp.zeros((heads, size), jnp.float32)
+        for k in range(key_heads):
+            total = jnp.where(head_rows // groups == k, rows[k : k + 1, :], total)
+        return total
+
+    own_score = (
+        jnp.sum(queries.astype(jnp.float32) * per_head(fresh_ref), axis=1, keepdims=True) * inv_root
+    )
+    logit_row = jnp.broadcast_to(forget_ref[...], (heads, heads))
+    diagonal = lax.broadcasted_iota(jnp.int32, (heads, heads), 1) == head_rows
+    logit = jnp.sum(jnp.where(diagonal, logit_row, 0.0), axis=1, keepdims=True)
+    log_gate = jnp.minimum(logit, 0.0) - jnp.log1p(jnp.exp(-jnp.abs(logit)))
+    cumlog_copy.wait()
+    positions = lax.broadcasted_iota(jnp.int32, (heads, span), 1)
+    latest = jnp.sum(
+        jnp.where(positions == length - 1, cumlog[...], 0.0), axis=1, keepdims=True
+    )
+    offset = latest + log_gate
+    scores = []
+    for c in range(chunk_count):
+        key_copies[c].wait()
+        block = jnp.concatenate(
+            [keys[k, c * step : (c + 1) * step, :] for k in range(key_heads)], axis=1
+        )
+        raw = lax.dot_general(wide, block, contract_last, preferred_element_type=jnp.float32)
+        raw = raw * inv_root + offset - cumlog[:, c * step : (c + 1) * step]
+        visible = positions[:, c * step : (c + 1) * step] < length
+        scores.append(jnp.where(visible, raw, -jnp.inf))
+    top = own_score
+    for part in scores:
+        top = jnp.maximum(top, jnp.max(part, axis=1, keepdims=True))
+    own_weight = jnp.exp(own_score - top)
+    denominator = own_weight
+    total = jnp.zeros((heads, key_heads * size), jnp.float32)
+    for c in range(chunk_count):
+        weights = jnp.exp(scores[c] - top)
+        denominator = denominator + jnp.sum(weights, axis=1, keepdims=True)
+        value_copies[c].wait()
+        block = jnp.concatenate(
+            [values[k, c * step : (c + 1) * step, :] for k in range(key_heads)], axis=1
+        )
+        total = total + jnp.dot(
+            weights.astype(jnp.bfloat16), block, preferred_element_type=jnp.float32
+        )
+    mine = own_weight.astype(jnp.bfloat16).astype(jnp.float32) * per_head(value_new_ref)
+    for k in range(key_heads):
+        mine = mine + jnp.where(
+            head_rows // groups == k, total[:, k * size : (k + 1) * size], 0.0
+        )
+    attended = (mine / denominator).astype(jnp.bfloat16)
+    for peer in range(out_ref.shape[0]):
+        out_ref[peer] = attended
+
+
+def projection_kernel(rows_ref, weight_ref, residual_ref, out_ref):
+    tokens, heads, size = rows_ref.shape
+    stacked = rows_ref[...].reshape(tokens * heads, size)
+    which = lax.broadcasted_iota(jnp.int32, (tokens * heads, 1), 0) % heads
+    wide = jnp.concatenate(
+        [jnp.where(which == h, stacked, jnp.zeros_like(stacked)) for h in range(heads)], axis=1
+    )
+    product = jnp.dot(wide, weight_ref[...], preferred_element_type=jnp.float32)
+    mixed = jnp.sum(product.reshape(tokens, heads, product.shape[1]), axis=1)
+    stream = (residual_ref[...].astype(jnp.float32) + mixed).astype(jnp.bfloat16)
+    for peer in range(out_ref.shape[0]):
+        out_ref[peer] = stream
+
+
+def silu_product(gate, up):
+    return gate / (1.0 + jnp.exp(-gate)) * up
+
+
+def expert_kernel(
+    expert_ref,
+    blocks_ref,
+    gain_ref,
+    routes_ref,
+    scores_ref,
+    gate_ref,
+    up_ref,
+    down_ref,
+    shared_gate_ref,
+    shared_up_ref,
+    out_ref,
+):
+    peers, tokens, width = blocks_ref.shape
+    wide = [blocks_ref[p].astype(jnp.float32) for p in range(peers)]
+    squares = wide[0] * wide[0]
+    for block in wide[1:]:
+        squares = squares + block * block
+    mean = jnp.sum(squares, axis=1, keepdims=True) / (peers * width)
+    inv_rms = lax.rsqrt(mean + norm_eps)
+    normed = jnp.concatenate(
+        [
+            (wide[p] * inv_rms * gain_ref[p : p + 1, :]).astype(jnp.bfloat16)
+            for p in range(peers)
+        ],
+        axis=1,
+    )
+    scores = scores_ref[...]
+    shares = scores / jnp.sum(scores, axis=0, keepdims=True) * routed_scale
+    share = jnp.sum(
+        jnp.where(routes_ref[...] == expert_ref[0], shares, 0.0), axis=0, keepdims=True
+    )
+
+    def against(matrix):
+        return lax.dot_general(matrix, normed, contract_last, preferred_element_type=jnp.float32)
+
+    shared_hidden = silu_product(against(shared_gate_ref[...]), against(shared_up_ref[...])).astype(
+        jnp.bfloat16
+    )
+    units = shared_hidden.shape[0]
+    spread = (
+        lax.broadcasted_iota(jnp.int32, (units, width), 0)
+        == lax.broadcasted_iota(jnp.int32, (units, width), 1)
+    ).astype(jnp.bfloat16)
+    contract_first = (((0,), (0,)), ((), ()))
+    shared_rows = lax.dot_general(
+        shared_hidden, spread, contract_first, preferred_element_type=jnp.float32
+    ).astype(jnp.bfloat16)
+    hidden = (silu_product(against(gate_ref[...]), against(up_ref[...])) * share).astype(
+        jnp.bfloat16
+    )
+    result = lax.dot_general(
+        hidden, down_ref[...], contract_first, preferred_element_type=jnp.float32
+    ).astype(jnp.bfloat16)
+    for p in range(peers):
+        out_ref[p, :tokens, :] = result[:, p * width : (p + 1) * width]
+        out_ref[p, tokens:, :] = shared_rows
+
+
+def combine_kernel(received_ref, stream_ref, down_ref, out_ref):
+    peers, double, width = received_ref.shape
+    tokens = double // 2
+    units = down_ref.shape[0] // peers
+    total = stream_ref[0].astype(jnp.float32)
+    for p in range(peers):
+        total = total + received_ref[p, :tokens, :].astype(jnp.float32)
+    for p in range(peers):
+        total = total + jnp.dot(
+            received_ref[p, tokens:, :][:, :units],
+            down_ref[p * units : (p + 1) * units, :],
+            preferred_element_type=jnp.float32,
+        )
+    out_ref[...] = total.astype(jnp.bfloat16)
+
+
+def exchange(blocks):
+    return lax.all_to_all(blocks, "ep", split_axis=0, concat_axis=0, tiled=True)
+
+
+def kernel_device(
+    queries,
+    fresh_token_key,
+    value_new,
+    forget_logit,
+    cache_keys,
+    cache_values,
+    cache_cumlog,
+    lengths,
+    residual,
+    out_weight,
+    norm_gain,
+    expert_gate,
+    expert_up,
+    expert_down,
+    shared_gate,
+    shared_up,
+    shared_down,
+    routes,
+    route_scores,
+):
+    peers = lax.axis_size("ep")
+    _, heads, size = queries.shape
+    _, key_heads, span, _ = cache_keys.shape
+    tokens, width = residual.shape
+    bf16 = jnp.bfloat16
+    spread = pl.pallas_call(
+        attention_kernel,
+        out_shape=jax.ShapeDtypeStruct((peers, heads, size), bf16),
+        in_specs=[pl.BlockSpec(memory_space=pltpu.SMEM)]
+        + [in_vmem()] * 4
+        + [pl.BlockSpec(memory_space=pl.ANY)] * 3,
+        out_specs=in_vmem(),
+        scratch_shapes=[
+            VMEM((key_heads, span, size), bf16),
+            VMEM((key_heads, span, size), bf16),
+            VMEM((heads, span), jnp.float32),
+            pltpu.SemaphoreType.DMA((2 * chunk_count + 1,)),
+        ],
+        compiler_params=params(12),
+        name="attention",
+    )(
+        lengths,
+        queries[0],
+        fresh_token_key[0],
+        value_new[0],
+        forget_logit,
+        cache_keys,
+        cache_values,
+        cache_cumlog,
+    )
+    rows = exchange(spread)
+    stream = pl.pallas_call(
+        projection_kernel,
+        out_shape=jax.ShapeDtypeStruct((peers, tokens, width), bf16),
+        in_specs=[in_vmem()] * 3,
+        out_specs=in_vmem(),
+        compiler_params=params(4),
+        name="projection",
+    )(rows, out_weight, residual)
+    blocks = exchange(stream)
+    expert = lax.axis_index("ep").reshape(1)
+    outgoing = pl.pallas_call(
+        expert_kernel,
+        out_shape=jax.ShapeDtypeStruct((peers, 2 * tokens, width), bf16),
+        in_specs=[pl.BlockSpec(memory_space=pltpu.SMEM)] + [in_vmem()] * 9,
+        out_specs=in_vmem(),
+        compiler_params=params(16),
+        name="experts",
+    )(
+        expert,
+        blocks,
+        norm_gain.reshape(peers, width),
+        routes.T,
+        route_scores.T,
+        expert_gate[0],
+        expert_up[0],
+        expert_down[0],
+        shared_gate,
+        shared_up,
+    )
+    received = exchange(outgoing)
+    return pl.pallas_call(
+        combine_kernel,
+        out_shape=jax.ShapeDtypeStruct((tokens, width), bf16),
+        in_specs=[in_vmem()] * 3,
+        out_specs=in_vmem(),
+        compiler_params=params(4),
+        name="combine",
+    )(received, stream, shared_down)
+
+
+def on_device(*arrays):
+    residual, expert_gate, shared_gate = arrays[8], arrays[11], arrays[14]
+    queries, cache_keys = arrays[0], arrays[4]
+    fits = (
+        residual.shape[1] % 128 == 0
+        and residual.shape[0] % 16 == 0
+        and shared_gate.shape[0] % 8 == 0
+        and shared_gate.shape[0] <= residual.shape[1]
+        and expert_gate.shape[0] == 1
+        and queries.shape[0] == 1
+        and cache_keys.shape[2] % (128 * chunk_count) == 0
+    )
+    return kernel_device(*arrays) if fits else plain_device(*arrays)
+
+
 def solution(mesh):
     placed = (
         P(("grp", "ep"), None, None),

time: 111 us -> 55.6 us (0.50)
  blocking collectives: 62.7 us -> 24.3 us
  other arithmetic: 17.8 us -> 0 us
  matrix products: 16.1 us -> 0 us
  Pallas kernels: 0 us -> 8.04 us
  waiting for transfers between devices: 0.01 us -> 6.86 us
  local copies, waits for them, and re-layouts: 9.72 us -> 11.4 us
    all_gather x3 -> x0, blocking collectives: 62.7 us -> none  [the longest x1 23.3 us: on_device(): lax.all_gather(attended, 'ep', axis=0, tiled=True)]
    all_to_all x0 -> x2, blocking collectives: none -> 24.3 us  [exchange(): return lax.all_to_all(blocks, 'ep', split_axis=0, concat_axis=0, tiled=True)]
    dot_general x11 -> x0, matrix products: 16.1 us -> none  [the longest x2 3.89 us: expert_hidden(): lax.dot_general(row_block, gate_matrix, contract_last, preferred_element_...]
    unnamed x2 -> x0, other arithmetic: 12.6 us -> none
    pallas_call x0 -> x4, Pallas kernels: none -> 8.04 us  [the longest x1 2.96 us: kernel_device(): pl.pallas_call(attention_kernel, out_shape=jax.ShapeDtypeStruct((peers, h...]
    all_to_all x1, waiting for transfers between devices: 0.01 us -> 6.86 us  [exchange(): return lax.all_to_all(blocks, 'ep', split_axis=0, concat_axis=0, tiled=True)]
    unnamed x17 -> x36, local copies, waits for them, and re-layouts: 4.7 us -> 11.4 us
    all_to_all x3 -> x0, local copies, waits for them, and re-layouts: 2.35 us -> none  [on_device(): lax.all_to_all(expert_out[None], 'ep', split_axis=2, concat_axis=0, tiled...]
  transfers between devices with their start and end apart: 1 -> 1, of which waited for: 0 -> 1; matrix products, arithmetic and copies ran while one was open for 4% -> 0% of each run, Pallas kernels for 0% -> 0%
where the time goes in v1:
time: 55.6 us; the launch traced here: 55.1 us
  blocking collectives  24.3 us (44%)
  local copies, waits for them, and re-layouts  11.4 us (21%)
  Pallas kernels  8.04 us (14%)
  waiting for transfers between devices  6.86 us (12%)
  starting transfers between devices  3.49 us (6%)
  between operations  0.89 us (2%)
    all_to_all x2, blocking collectives, exchange(): return lax.all_to_all(blocks, 'ep', split_axis=0, concat_axis=0, tiled=True)  24.3 us
    unnamed x36, local copies, waits for them, and re-layouts  11.4 us
    all_to_all x1, waiting for transfers between devices, exchange(): return lax.all_to_all(blocks, 'ep', split_axis=0, concat_axis=0, tiled=True)  6.86 us
    all_to_all x1, starting transfers between devices, exchange(): return lax.all_to_all(blocks, 'ep', split_axis=0, concat_axis=0, tiled=True)  3.49 us
    pallas_call x1, Pallas kernels, kernel_device(): pl.pallas_call(attention_kernel, out_shape=jax.ShapeDtypeStruct((peers, h...  2.96 us
    pallas_call x1, Pallas kernels, kernel_device(): pl.pallas_call(expert_kernel, out_shape=jax.ShapeDtypeStruct((peers, 2 *...  2.55 us
    pallas_call x1, Pallas kernels, kernel_device(): pl.pallas_call(combine_kernel, out_shape=jax.ShapeDtypeStruct((tokens, wi...  1.66 us
  transfers between devices with their start and end apart: 1, of which 1 were waited for; matrix products, arithmetic and copies ran while one was open for 0% of the time, Pallas kernels for 0%

profile of v1, /device:TPU:0, one launch (start us, length us, event | category | flops | bytes accessed | tf_op | source)
XLA Modules:
  0.0 55.1 jit_solution(7187150938665869147)
XLA Ops:
  0.0 0.0 copy-start
  0.8 0.0 copy-start.3
  0.8 1.7 %copy-done.3 = bf16[1,2,4096,128]{3,2,1,0:T(8,128)(2,1)S(1)} copy-done((bf16[1,2,4096,128]{3,2,1,0:T(8,128)(2,1)S(1)}, bf16[1,2,4096,128]{3,2,1,0:T(8,128)(2,1)}, u32[]{:S(2)}) %copy-start.3) | copy-done | bytes 2097176
  2.5 0.0 copy-start.4
  2.5 1.6 %copy-done.4 = bf16[1,2,4096,128]{3,2,1,0:T(8,128)(2,1)S(1)} copy-done((bf16[1,2,4096,128]{3,2,1,0:T(8,128)(2,1)S(1)}, bf16[1,2,4096,128]{3,2,1,0:T(8,128)(2,1)}, u32[]{:S(2)}) %copy-start.4) | copy-done | bytes 2097176
  4.1 0.0 copy-start.9
  4.1 0.9 %copy-done.9 = f32[1,8,4096]{2,1,0:T(8,128)S(1)} copy-done((f32[1,8,4096]{2,1,0:T(8,128)S(1)}, f32[1,8,4096]{2,1,0:T(8,128)}, u32[]{:S(2)}) %copy-start.9) | copy-done | bytes 131096
  5.0 0.0 copy-start.14
  5.0 0.7 %copy-done.14 = bf16[1,8,128]{2,1,0:T(8,128)(2,1)S(1)} copy-done((bf16[1,8,128]{2,1,0:T(8,128)(2,1)S(1)}, bf16[1,8,128]{2,1,0:T(8,128)(2,1)}, u32[]{:S(2)}) %copy-start.14) | copy-done | bytes 2072
  5.7 0.0 copy-start.15
  5.7 0.7 %copy-done.15 = bf16[1,2,128]{2,1,0:T(2,128)(2,1)S(1)} copy-done((bf16[1,2,128]{2,1,0:T(2,128)(2,1)S(1)}, bf16[1,2,128]{2,1,0:T(2,128)(2,1)}, u32[]{:S(2)}) %copy-start.15) | copy-done | bytes 536
  6.3 0.0 copy-start.16
  6.3 0.7 %copy-done.16 = bf16[1,2,128]{2,1,0:T(2,128)(2,1)S(1)} copy-done((bf16[1,2,128]{2,1,0:T(2,128)(2,1)S(1)}, bf16[1,2,128]{2,1,0:T(2,128)(2,1)}, u32[]{:S(2)}) %copy-start.16) | copy-done | bytes 536
  7.0 0.0 copy-start.17
  7.0 0.7 %copy-done.17 = f32[1,8]{1,0:T(1,128)S(1)} copy-done((f32[1,8]{1,0:T(1,128)S(1)}, f32[1,8]{1,0:T(1,128)}, u32[]{:S(2)}) %copy-start.17) | copy-done | bytes 56
  7.6 0.0 copy-start.8
  7.6 0.0 copy-start.13
  7.6 0.0 copy-start.5
  7.6 0.0 copy-start.10
  7.6 0.0 copy-start.11
  7.6 0.0 copy-start.12
  7.7 3.0 %attention.1 = bf16[16,8,128]{2,1,0:T(8,128)(2,1)S(1)} custom-call(s32[1]{0:T(128)S(6)} %copy.20.lengths_ref, bf16[8,128]{1,0:T(8,128)(2,1)S(1)} %bitcast.16, bf16[2,128]{1,0:T(2,128)(2,1)S(1)} %bitcast.17, bf16[2,128]{1,0:T(2,128)(2,1)S(1)} %bitcast.18, f32[1,8]{1,0:T(1,128)S(1)} %copy-done.17, bf16[1,2,4096,128]{3,2,1,0:T(8,128)(2,1)S(1)} %copy-done.3, ...), custom_call_target="tpu_custom_call" | custom-call | tf_op jit(solution)/shard_map/attention/pallas_call | solution.py:398
  10.6 13.8 %all_to_all.15.rows_ref = bf16[16,8,128]{2,1,0:T(8,128)(2,1)S(1)} all-to-all(bf16[16,8,128]{2,1,0:T(8,128)(2,1)S(1)} %attention.1), channel_id=1, replica_groups=mesh['grp'=2,'ep'=16] {'ep'}, dimensions={0} | all-to-all | bytes 65536 | tf_op jit(solution)/shard_map/all_to_all | solution.py:369
  24.5 0.0 copy-done.8
  24.5 0.0 copy-done.13
  24.5 0.9 %projection.1.stream_ref = bf16[16,16,128]{2,1,0:T(8,128)(2,1)} custom-call(bf16[16,8,128]{2,1,0:T(8,128)(2,1)S(1)} %all_to_all.15.rows_ref, bf16[1024,128]{1,0:T(8,128)(2,1)S(1)} %copy-done.8, bf16[16,128]{1,0:T(8,128)(2,1)S(1)} %copy-done.13), custom_call_target="tpu_custom_call" | custom-call | tf_op jit(solution)/shard_map/projection/pallas_call | solution.py:424
  25.3 3.5 %all-to-all-start.1 = ((bf16[16,16,128]{2,1,0:T(8,128)(2,1)}), bf16[16,16,128]{2,1,0:T(8,128)(2,1)S(1)}, u32[]{:S(2)}, u32[]{:S(2)}) async-start(bf16[16,16,128]{2,1,0:T(8,128)(2,1)} %projection.1.stream_ref), calls=%async_computation.1 | async-start | bytes 131072 | tf_op jit(solution)/shard_map/all_to_all | solution.py:369
  28.8 6.9 %all-to-all-done.1.blocks_ref = bf16[16,16,128]{2,1,0:T(8,128)(2,1)S(1)} async-done(((bf16[16,16,128]{2,1,0:T(8,128)(2,1)}), bf16[16,16,128]{2,1,0:T(8,128)(2,1)S(1)}, u32[]{:S(2)}, u32[]{:S(2)}) %all-to-all-start.1) | async-done | bytes 65568 | tf_op jit(solution)/shard_map/all_to_all | solution.py:369
  35.7 0.0 copy-done
  35.7 0.0 copy-done.5
  35.7 0.0 copy-done.10
  35.7 0.0 copy-done.11
  35.7 0.0 copy-done.12
  35.7 0.0 copy-start.1
  35.7 1.8 %copy-done.1 = bf16[1,704,2048]{2,1,0:T(8,128)(2,1)S(1)} copy-done((bf16[1,704,2048]{2,1,0:T(8,128)(2,1)S(1)}, bf16[1,704,2048]{2,1,0:T(8,128)(2,1)}, u32[]{:S(2)}) %copy-start.1) | copy-done | bytes 2883608
  37.6 0.0 copy-start.2
  37.6 1.8 %copy-done.2 = bf16[1,704,2048]{2,1,0:T(8,128)(2,1)S(1)} copy-done((bf16[1,704,2048]{2,1,0:T(8,128)(2,1)S(1)}, bf16[1,704,2048]{2,1,0:T(8,128)(2,1)}, u32[]{:S(2)}) %copy-start.2) | copy-done | bytes 2883608
  39.4 0.0 copy-start.6
  39.4 1.0 %copy-done.6 = bf16[88,2048]{1,0:T(8,128)(2,1)S(1)} copy-done((bf16[88,2048]{1,0:T(8,128)(2,1)S(1)}, bf16[88,2048]{1,0:T(8,128)(2,1)}, u32[]{:S(2)}) %copy-start.6) | copy-done | bytes 360472
  40.4 0.0 copy-start.7
  40.4 2.6 %experts.1 = bf16[16,32,128]{2,1,0:T(8,128)(2,1)S(1)} custom-call(s32[1]{0:T(128)} %bitcast.expert_ref, bf16[16,16,128]{2,1,0:T(8,128)(2,1)S(1)} %all-to-all-done.1.blocks_ref, f32[16,128]{1,0:T(8,128)S(1)} %bitcast.13, s32[6,16]{1,0:T(8,128)S(1)} %bitcast.14, f32[6,16]{1,0:T(8,128)S(1)} %bitcast.15, bf16[704,2048]{1,0:T(8,128)(2,1)S(1)} %bitcast.10, ...), custom_call_target="tpu_custom_call" | custom-call | tf_op jit(solution)/shard_map/experts/pallas_call | solution.py:434
  42.9 10.5 %all_to_all.16.received_ref = bf16[16,32,128]{2,1,0:T(8,128)(2,1)S(1)} all-to-all(bf16[16,32,128]{2,1,0:T(8,128)(2,1)S(1)} %experts.1), channel_id=1, replica_groups=mesh['grp'=2,'ep'=16] {'ep'}, dimensions={0} | all-to-all | bytes 262144 | tf_op jit(solution)/shard_map/all_to_all | solution.py:369
  53.4 0.0 copy-done.7
  53.4 1.7 %combine.1 = bf16[16,128]{1,0:T(8,128)(2,1)} custom-call(bf16[16,32,128]{2,1,0:T(8,128)(2,1)S(1)} %all_to_all.16.received_ref, bf16[16,16,128]{2,1,0:T(8,128)(2,1)} %projection.1.stream_ref, bf16[1408,128]{1,0:T(8,128)(2,1)S(1)} %copy-done.7), custom_call_target="tpu_custom_call" | custom-call | tf_op jit(solution)/shard_map/combine/pallas_call | solution.py:454
Async XLA Ops:
  0.0 35.7 %copy-start = (bf16[1,704,2048]{2,1,0:T(8,128)(2,1)S(1)}, bf16[1,704,2048]{2,1,0:T(8,128)(2,1)}, u32[]{:S(2)}) copy-start(bf16[1,704,2048]{2,1,0:T(8,128)(2,1)} %param.30) | copy-start | bytes 8650756
  0.8 1.7 %copy-start.3 = (bf16[1,2,4096,128]{3,2,1,0:T(8,128)(2,1)S(1)}, bf16[1,2,4096,128]{3,2,1,0:T(8,128)(2,1)}, u32[]{:S(2)}) copy-start(bf16[1,2,4096,128]{3,2,1,0:T(8,128)(2,1)} %keys_hbm.1) | copy-start | bytes 6291460
  2.5 1.6 %copy-start.4 = (bf16[1,2,4096,128]{3,2,1,0:T(8,128)(2,1)S(1)}, bf16[1,2,4096,128]{3,2,1,0:T(8,128)(2,1)}, u32[]{:S(2)}) copy-start(bf16[1,2,4096,128]{3,2,1,0:T(8,128)(2,1)} %values_hbm.1) | copy-start | bytes 6291460
  4.1 0.9 %copy-start.9 = (f32[1,8,4096]{2,1,0:T(8,128)S(1)}, f32[1,8,4096]{2,1,0:T(8,128)}, u32[]{:S(2)}) copy-start(f32[1,8,4096]{2,1,0:T(8,128)} %cumlog_hbm.1) | copy-start | bytes 393220
  5.0 0.7 %copy-start.14 = (bf16[1,8,128]{2,1,0:T(8,128)(2,1)S(1)}, bf16[1,8,128]{2,1,0:T(8,128)(2,1)}, u32[]{:S(2)}) copy-start(bf16[1,8,128]{2,1,0:T(8,128)(2,1)} %param.19) | copy-start | bytes 6148
  5.7 0.7 %copy-start.15 = (bf16[1,2,128]{2,1,0:T(2,128)(2,1)S(1)}, bf16[1,2,128]{2,1,0:T(2,128)(2,1)}, u32[]{:S(2)}) copy-start(bf16[1,2,128]{2,1,0:T(2,128)(2,1)} %param.20) | copy-start | bytes 1540
  6.3 0.7 %copy-start.16 = (bf16[1,2,128]{2,1,0:T(2,128)(2,1)S(1)}, bf16[1,2,128]{2,1,0:T(2,128)(2,1)}, u32[]{:S(2)}) copy-start(bf16[1,2,128]{2,1,0:T(2,128)(2,1)} %param.21) | copy-start | bytes 1540
  7.0 0.7 %copy-start.17 = (f32[1,8]{1,0:T(1,128)S(1)}, f32[1,8]{1,0:T(1,128)}, u32[]{:S(2)}) copy-start(f32[1,8]{1,0:T(1,128)} %forget_ref.1) | copy-start | bytes 100
  7.6 16.9 %copy-start.8 = (bf16[1024,128]{1,0:T(8,128)(2,1)S(1)}, bf16[1024,128]{1,0:T(8,128)(2,1)}, u32[]{:S(2)}) copy-start(bf16[1024,128]{1,0:T(8,128)(2,1)} %weight_ref.1) | copy-start | bytes 786436
  7.6 16.9 %copy-start.13 = (bf16[16,128]{1,0:T(8,128)(2,1)S(1)}, bf16[16,128]{1,0:T(8,128)(2,1)}, u32[]{:S(2)}) copy-start(bf16[16,128]{1,0:T(8,128)(2,1)} %residual_ref.1) | copy-start | bytes 12292
  7.6 28.1 %copy-start.5 = (bf16[88,2048]{1,0:T(8,128)(2,1)S(1)}, bf16[88,2048]{1,0:T(8,128)(2,1)}, u32[]{:S(2)}) copy-start(bf16[88,2048]{1,0:T(8,128)(2,1)} %shared_gate_ref.1) | copy-start | bytes 1081348
  7.6 28.1 %copy-start.10 = (f32[2048]{0:T(1024)S(1)}, f32[2048]{0:T(1024)}, u32[]{:S(2)}) copy-start(f32[2048]{0:T(1024)} %param.29) | copy-start | bytes 24580
  7.6 28.1 %copy-start.11 = (s32[16,6]{0,1:T(8,128)S(1)}, s32[16,6]{0,1:T(8,128)}, u32[]{:S(2)}) copy-start(s32[16,6]{0,1:T(8,128)} %param.36) | copy-start | bytes 1156
  7.6 28.1 %copy-start.12 = (f32[16,6]{0,1:T(8,128)S(1)}, f32[16,6]{0,1:T(8,128)}, u32[]{:S(2)}) copy-start(f32[16,6]{0,1:T(8,128)} %param.37) | copy-start | bytes 1156
  25.3 10.4 %all-to-all-start.1 = ((bf16[16,16,128]{2,1,0:T(8,128)(2,1)}), bf16[16,16,128]{2,1,0:T(8,128)(2,1)S(1)}, u32[]{:S(2)}, u32[]{:S(2)}) async-start(bf16[16,16,128]{2,1,0:T(8,128)(2,1)} %projection.1.stream_ref), calls=%async_computation.1 | async-start | bytes 131072 | tf_op jit(solution)/shard_map/all_to_all | solution.py:369
  35.7 1.8 %copy-start.1 = (bf16[1,704,2048]{2,1,0:T(8,128)(2,1)S(1)}, bf16[1,704,2048]{2,1,0:T(8,128)(2,1)}, u32[]{:S(2)}) copy-start(bf16[1,704,2048]{2,1,0:T(8,128)(2,1)} %param.31) | copy-start | bytes 8650756
  37.6 1.8 %copy-start.2 = (bf16[1,704,2048]{2,1,0:T(8,128)(2,1)S(1)}, bf16[1,704,2048]{2,1,0:T(8,128)(2,1)}, u32[]{:S(2)}) copy-start(bf16[1,704,2048]{2,1,0:T(8,128)(2,1)} %param.32) | copy-start | bytes 8650756
  39.4 1.0 %copy-start.6 = (bf16[88,2048]{1,0:T(8,128)(2,1)S(1)}, bf16[88,2048]{1,0:T(8,128)(2,1)}, u32[]{:S(2)}) copy-start(bf16[88,2048]{1,0:T(8,128)(2,1)} %shared_up_ref.1) | copy-start | bytes 1081348
  40.4 13.1 %copy-start.7 = (bf16[1408,128]{1,0:T(8,128)(2,1)S(1)}, bf16[1408,128]{1,0:T(8,128)(2,1)}, u32[]{:S(2)}) copy-start(bf16[1408,128]{1,0:T(8,128)(2,1)} %down_ref.1) | copy-start | bytes 1081348

commit v2 on v1

--- a/solution.py
+++ b/solution.py
@@ -166,20 +166,32 @@
     return pl.BlockSpec(memory_space=VMEM)
 
 
+def in_hbm():
+    return pl.BlockSpec(memory_space=pltpu.HBM)
+
+
+def held_in_hbm(*arrays):
+    return [pltpu.with_memory_space_constraint(a, pltpu.HBM) for a in arrays]
+
+
 def params(mib):
     return pltpu.CompilerParams(vmem_limit_bytes=mib * 1024 * 1024)
 
 
 def attention_kernel(
     lengths_ref,
+    queries_hbm,
+    fresh_hbm,
+    value_new_hbm,
+    forget_hbm,
+    keys_hbm,
+    values_hbm,
+    cumlog_hbm,
+    out_ref,
     queries_ref,
     fresh_ref,
     value_new_ref,
     forget_ref,
-    keys_hbm,
-    values_hbm,
-    cumlog_hbm,
-    out_ref,
     keys,
     values,
     cumlog,
@@ -190,8 +202,20 @@
     groups = heads // key_heads
     step = span // chunk_count
     inv_root = size ** (-0.5)
-    cumlog_copy = pltpu.make_async_copy(cumlog_hbm.at[0], cumlog, sems.at[2 * chunk_count])
-    cumlog_copy.start()
+    small_copies = [
+        pltpu.make_async_copy(source, target, sems.at[2 * chunk_count + i])
+        for i, (source, target) in enumerate(
+            (
+                (queries_hbm.at[0], queries_ref),
+                (fresh_hbm.at[0], fresh_ref),
+                (forget_hbm, forget_ref),
+                (value_new_hbm.at[0], value_new_ref),
+                (cumlog_hbm.at[0], cumlog),
+            )
+        )
+    ]
+    for copy in small_copies:
+        copy.start()
 
     def copies(source, target, first):
         return [
@@ -209,6 +233,8 @@
         copy.start()
 
     length = lengths_ref[0]
+    for copy in small_copies[:-1]:
+        copy.wait()
     queries = queries_ref[...]
     head_rows = lax.broadcasted_iota(jnp.int32, (heads, 1), 0)
     wide = jnp.concatenate(
@@ -230,7 +256,7 @@
     diagonal = lax.broadcasted_iota(jnp.int32, (heads, heads), 1) == head_rows
     logit = jnp.sum(jnp.where(diagonal, logit_row, 0.0), axis=1, keepdims=True)
     log_gate = jnp.minimum(logit, 0.0) - jnp.log1p(jnp.exp(-jnp.abs(logit)))
-    cumlog_copy.wait()
+    small_copies[-1].wait()
     positions = lax.broadcasted_iota(jnp.int32, (heads, span), 1)
     latest = jnp.sum(
         jnp.where(positions == length - 1, cumlog[...], 0.0), axis=1, keepdims=True
@@ -291,7 +317,6 @@
 
 
 def expert_kernel(
-    expert_ref,
     blocks_ref,
     gain_ref,
     routes_ref,
@@ -320,7 +345,7 @@
     scores = scores_ref[...]
     shares = scores / jnp.sum(scores, axis=0, keepdims=True) * routed_scale
     share = jnp.sum(
-        jnp.where(routes_ref[...] == expert_ref[0], shares, 0.0), axis=0, keepdims=True
+        jnp.where(routes_ref[...] == lax.axis_index("ep"), shares, 0.0), axis=0, keepdims=True
     )
 
     def against(matrix):
@@ -397,58 +422,60 @@
     bf16 = jnp.bfloat16
     spread = pl.pallas_call(
         attention_kernel,
-        out_shape=jax.ShapeDtypeStruct((peers, heads, size), bf16),
-        in_specs=[pl.BlockSpec(memory_space=pltpu.SMEM)]
-        + [in_vmem()] * 4
-        + [pl.BlockSpec(memory_space=pl.ANY)] * 3,
+        out_shape=VMEM((peers, heads, size), bf16),
+        in_specs=[pl.BlockSpec(memory_space=pltpu.SMEM)] + [in_hbm()] * 7,
         out_specs=in_vmem(),
         scratch_shapes=[
+            VMEM((heads, size), bf16),
+            VMEM((key_heads, size), bf16),
+            VMEM((key_heads, size), bf16),
+            VMEM((1, heads), jnp.float32),
             VMEM((key_heads, span, size), bf16),
             VMEM((key_heads, span, size), bf16),
             VMEM((heads, span), jnp.float32),
-            pltpu.SemaphoreType.DMA((2 * chunk_count + 1,)),
+            pltpu.SemaphoreType.DMA((2 * chunk_count + 5,)),
         ],
         compiler_params=params(12),
         name="attention",
     )(
         lengths,
-        queries[0],
-        fresh_token_key[0],
-        value_new[0],
-        forget_logit,
-        cache_keys,
-        cache_values,
-        cache_cumlog,
+        *held_in_hbm(
+            queries,
+            fresh_token_key,
+            value_new,
+            forget_logit,
+            cache_keys,
+            cache_values,
+            cache_cumlog,
+        ),
     )
     rows = exchange(spread)
     stream = pl.pallas_call(
         projection_kernel,
-        out_shape=jax.ShapeDtypeStruct((peers, tokens, width), bf16),
+        out_shape=VMEM((peers, tokens, width), bf16),
         in_specs=[in_vmem()] * 3,
         out_specs=in_vmem(),
         compiler_params=params(4),
+        cost_estimate=pl.CostEstimate(flops=100000000000, bytes_accessed=0, transcendentals=0),
         name="projection",
     )(rows, out_weight, residual)
     blocks = exchange(stream)
-    expert = lax.axis_index("ep").reshape(1)
     outgoing = pl.pallas_call(
         expert_kernel,
-        out_shape=jax.ShapeDtypeStruct((peers, 2 * tokens, width), bf16),
-        in_specs=[pl.BlockSpec(memory_space=pltpu.SMEM)] + [in_vmem()] * 9,
+        out_shape=VMEM((peers, 2 * tokens, width), bf16),
+        in_specs=[in_vmem()] * 9,
         out_specs=in_vmem(),
         compiler_params=params(16),
         name="experts",
     )(
-        expert,
         blocks,
         norm_gain.reshape(peers, width),
         routes.T,
         route_scores.T,
-        expert_gate[0],
-        expert_up[0],
-        expert_down[0],
-        shared_gate,
-        shared_up,
+        *(
+            pltpu.with_memory_space_constraint(a, VMEM)
+            for a in (expert_gate[0], expert_up[0], expert_down[0], shared_gate, shared_up)
+        ),
     )
     received = exchange(outgoing)
     return pl.pallas_call(

time: 55.6 us -> 42.6 us (0.77)
  local copies, waits for them, and re-layouts: 11.4 us -> 0.06 us
  blocking collectives: 24.3 us -> 34.3 us
  waiting for transfers between devices: 6.86 us -> 0 us
  starting transfers between devices: 3.49 us -> 0 us
  Pallas kernels: 8.04 us -> 7.1 us
    unnamed x36 -> x22, local copies, waits for them, and re-layouts: 11.4 us -> 0.06 us
    all_to_all x2 -> x3, blocking collectives: 24.3 us -> 34.3 us  [exchange(): return lax.all_to_all(blocks, 'ep', split_axis=0, concat_axis=0, tiled=True)]
    all_to_all x1 -> x0, waiting for transfers between devices: 6.86 us -> none  [exchange(): return lax.all_to_all(blocks, 'ep', split_axis=0, concat_axis=0, tiled=True)]
    all_to_all x1 -> x0, starting transfers between devices: 3.49 us -> none  [exchange(): return lax.all_to_all(blocks, 'ep', split_axis=0, concat_axis=0, tiled=True)]
    pallas_call x1, Pallas kernels: 1.66 us -> 0.82 us  [kernel_device(): pl.pallas_call(combine_kernel, out_shape=jax.ShapeDtypeStruct((tokens, wi...]
  transfers between devices with their start and end apart: 1 -> 0, of which waited for: 1 -> 0; matrix products, arithmetic and copies ran while one was open for 0% -> 0% of each run, Pallas kernels for 0% -> 0%
where the time goes in v2:
time: 42.6 us; the launch traced here: 42.3 us
  blocking collectives  34.3 us (81%)
  Pallas kernels  7.1 us (17%)
  between operations  0.82 us (2%)
    all_to_all x3, blocking collectives, exchange(): return lax.all_to_all(blocks, 'ep', split_axis=0, concat_axis=0, tiled=True)  34.3 us
    pallas_call x1, Pallas kernels, kernel_device(): pl.pallas_call(attention_kernel, out_shape=VMEM((peers, heads, size), bf1...  3.5 us
    pallas_call x1, Pallas kernels, kernel_device(): pl.pallas_call(expert_kernel, out_shape=VMEM((peers, 2 * tokens, width),...  2.55 us

profile of v2, /device:TPU:0, one launch (start us, length us, event | category | flops | bytes accessed | tf_op | source)
XLA Modules:
  0.0 42.3 jit_solution(2630675537272210367)
XLA Ops:
  0.0 0.0 copy-start.9
  0.0 0.0 copy-start.10
  0.7 3.5 %attention.1 = bf16[16,8,128]{2,1,0:T(8,128)(2,1)S(1)} custom-call(s32[1]{0:T(128)S(6)} %copy.20.lengths_ref, bf16[1,8,128]{2,1,0:T(8,128)(2,1)} %queries_hbm.1, bf16[1,2,128]{2,1,0:T(2,128)(2,1)} %fresh_hbm.1, bf16[1,2,128]{2,1,0:T(2,128)(2,1)} %value_new_hbm.1, f32[1,8]{1,0:T(1,128)} %forget_hbm.1, bf16[1,2,4096,128]{3,2,1,0:T(8,128)(2,1)} %keys_hbm.1, ...), custom_call_target="tpu_custom_call" | custom-call | tf_op jit(solution)/shard_map/attention/pallas_call | solution.py:423
  4.2 13.8 %all_to_all.15.rows_ref = bf16[16,8,128]{2,1,0:T(8,128)(2,1)S(1)} all-to-all(bf16[16,8,128]{2,1,0:T(8,128)(2,1)S(1)} %attention.1), channel_id=1, replica_groups=mesh['grp'=2,'ep'=16] {'ep'}, dimensions={0} | all-to-all | bytes 65536 | tf_op jit(solution)/shard_map/all_to_all | solution.py:394
  18.1 0.0 copy-done.9
  18.1 0.0 copy-done.10
  18.1 0.0 copy-start
  18.1 0.0 copy-start.1
  18.1 0.0 copy-start.2
  18.1 0.0 copy-start.3
  18.1 0.0 copy-start.4
  18.1 0.0 copy-start.6
  18.1 0.0 copy-start.7
  18.1 0.0 copy-start.8
  18.1 0.2 projection.1.stream_ref
  18.4 10.0 %all_to_all.16.blocks_ref = bf16[16,16,128]{2,1,0:T(8,128)(2,1)S(1)} all-to-all(bf16[16,16,128]{2,1,0:T(8,128)(2,1)S(1)} %projection.1.stream_ref), channel_id=1, replica_groups=mesh['grp'=2,'ep'=16] {'ep'}, dimensions={0} | all-to-all | bytes 131072 | tf_op jit(solution)/shard_map/all_to_all | solution.py:394
  28.4 0.0 copy-done
  28.4 0.0 copy-done.1
  28.4 0.0 copy-done.2
  28.4 0.0 copy-done.3
  28.4 0.0 copy-done.4
  28.4 0.0 copy-done.6
  28.4 0.0 copy-done.7
  28.4 0.0 copy-done.8
  28.4 0.0 copy-start.5
  28.5 2.5 %experts.1 = bf16[16,32,128]{2,1,0:T(8,128)(2,1)S(1)} custom-call(bf16[16,16,128]{2,1,0:T(8,128)(2,1)S(1)} %all_to_all.16.blocks_ref, f32[16,128]{1,0:T(8,128)S(1)} %bitcast.9, s32[6,16]{1,0:T(8,128)S(1)} %bitcast.10, f32[6,16]{1,0:T(8,128)S(1)} %bitcast.11, bf16[704,2048]{1,0:T(8,128)(2,1)S(1)} %bitcast.6, bf16[704,2048]{1,0:T(8,128)(2,1)S(1)} %bitcast.7, ...), custom_call_target="tpu_custom_call" | custom-call | tf_op jit(solution)/shard_map/experts/pallas_call | solution.py:463
  31.0 10.5 %all_to_all.17.received_ref = bf16[16,32,128]{2,1,0:T(8,128)(2,1)S(1)} all-to-all(bf16[16,32,128]{2,1,0:T(8,128)(2,1)S(1)} %experts.1), channel_id=1, replica_groups=mesh['grp'=2,'ep'=16] {'ep'}, dimensions={0} | all-to-all | bytes 262144 | tf_op jit(solution)/shard_map/all_to_all | solution.py:394
  41.5 0.0 copy-done.5
  41.5 0.8 %combine.1 = bf16[16,128]{1,0:T(8,128)(2,1)} custom-call(bf16[16,32,128]{2,1,0:T(8,128)(2,1)S(1)} %all_to_all.17.received_ref, bf16[16,16,128]{2,1,0:T(8,128)(2,1)S(1)} %projection.1.stream_ref, bf16[1408,128]{1,0:T(8,128)(2,1)S(1)} %copy-done.5), custom_call_target="tpu_custom_call" | custom-call | tf_op jit(solution)/shard_map/combine/pallas_call | solution.py:481
Async XLA Ops:
  0.0 18.1 %copy-start.9 = (bf16[1024,128]{1,0:T(8,128)(2,1)S(1)}, bf16[1024,128]{1,0:T(8,128)(2,1)}, u32[]{:S(2)}) copy-start(bf16[1024,128]{1,0:T(8,128)(2,1)} %weight_ref.1) | copy-start | bytes 786436
  0.0 18.1 %copy-start.10 = (bf16[16,128]{1,0:T(8,128)(2,1)S(1)}, bf16[16,128]{1,0:T(8,128)(2,1)}, u32[]{:S(2)}) copy-start(bf16[16,128]{1,0:T(8,128)(2,1)} %residual_ref.1) | copy-start | bytes 12292
  18.1 10.3 %copy-start = (bf16[1,704,2048]{2,1,0:T(8,128)(2,1)S(1)}, bf16[1,704,2048]{2,1,0:T(8,128)(2,1)}, u32[]{:S(2)}) copy-start(bf16[1,704,2048]{2,1,0:T(8,128)(2,1)} %param.30) | copy-start | bytes 8650756
  18.1 10.3 %copy-start.1 = (bf16[1,704,2048]{2,1,0:T(8,128)(2,1)S(1)}, bf16[1,704,2048]{2,1,0:T(8,128)(2,1)}, u32[]{:S(2)}) copy-start(bf16[1,704,2048]{2,1,0:T(8,128)(2,1)} %param.31) | copy-start | bytes 8650756
  18.1 10.3 %copy-start.2 = (bf16[1,704,2048]{2,1,0:T(8,128)(2,1)S(1)}, bf16[1,704,2048]{2,1,0:T(8,128)(2,1)}, u32[]{:S(2)}) copy-start(bf16[1,704,2048]{2,1,0:T(8,128)(2,1)} %param.32) | copy-start | bytes 8650756
  18.1 10.3 %copy-start.3 = (bf16[88,2048]{1,0:T(8,128)(2,1)S(1)}, bf16[88,2048]{1,0:T(8,128)(2,1)}, u32[]{:S(2)}) copy-start(bf16[88,2048]{1,0:T(8,128)(2,1)} %shared_gate_ref.1) | copy-start | bytes 1081348
  18.1 10.3 %copy-start.4 = (bf16[88,2048]{1,0:T(8,128)(2,1)S(1)}, bf16[88,2048]{1,0:T(8,128)(2,1)}, u32[]{:S(2)}) copy-start(bf16[88,2048]{1,0:T(8,128)(2,1)} %shared_up_ref.1) | copy-start | bytes 1081348
  18.1 10.3 %copy-start.6 = (f32[2048]{0:T(1024)S(1)}, f32[2048]{0:T(1024)}, u32[]{:S(2)}) copy-start(f32[2048]{0:T(1024)} %param.29) | copy-start | bytes 24580
  18.1 10.3 %copy-start.7 = (s32[16,6]{0,1:T(8,128)S(1)}, s32[16,6]{0,1:T(8,128)}, u32[]{:S(2)}) copy-start(s32[16,6]{0,1:T(8,128)} %param.36) | copy-start | bytes 1156
  18.1 10.3 %copy-start.8 = (f32[16,6]{0,1:T(8,128)S(1)}, f32[16,6]{0,1:T(8,128)}, u32[]{:S(2)}) copy-start(f32[16,6]{0,1:T(8,128)} %param.37) | copy-start | bytes 1156
  28.4 13.1 %copy-start.5 = (bf16[1408,128]{1,0:T(8,128)(2,1)S(1)}, bf16[1408,128]{1,0:T(8,128)(2,1)}, u32[]{:S(2)}) copy-start(bf16[1408,128]{1,0:T(8,128)(2,1)} %down_ref.1) | copy-start | bytes 1081348

commit v3 on v2

--- a/solution.py
+++ b/solution.py
@@ -159,7 +159,8 @@
 
 
 VMEM = pltpu.VMEM
-chunk_count = 4
+key_cuts = (0, 1, 4)
+value_cuts = (0, 4)
 
 
 def in_vmem():
@@ -194,53 +195,50 @@
     forget_ref,
     keys,
     values,
-    cumlog,
+    scores,
     sems,
 ):
     heads, size = queries_ref.shape
     key_heads, span, _ = keys.shape
     groups = heads // key_heads
-    step = span // chunk_count
     inv_root = size ** (-0.5)
+    first = len(key_cuts) + len(value_cuts) - 2
     small_copies = [
-        pltpu.make_async_copy(source, target, sems.at[2 * chunk_count + i])
+        pltpu.make_async_copy(source, target, sems.at[first + i])
         for i, (source, target) in enumerate(
             (
+                (cumlog_hbm.at[0], scores),
                 (queries_hbm.at[0], queries_ref),
                 (fresh_hbm.at[0], fresh_ref),
                 (forget_hbm, forget_ref),
                 (value_new_hbm.at[0], value_new_ref),
-                (cumlog_hbm.at[0], cumlog),
             )
         )
     ]
-    for copy in small_copies:
-        copy.start()
-
-    def copies(source, target, first):
+
+    def pieces(cuts):
+        edges = [span * cut // cuts[-1] for cut in cuts]
+        return list(zip(edges[:-1], edges[1:]))
+
+    def copies(source, target, cuts, first):
         return [
             pltpu.make_async_copy(
-                source.at[0, :, pl.ds(c * step, step), :],
-                target.at[:, pl.ds(c * step, step), :],
-                sems.at[first + c],
+                source.at[0, :, pl.ds(low, high - low), :],
+                target.at[:, pl.ds(low, high - low), :],
+                sems.at[first + i],
             )
-            for c in range(chunk_count)
+            for i, (low, high) in enumerate(pieces(cuts))
         ]
 
-    key_copies = copies(keys_hbm, keys, 0)
-    value_copies = copies(values_hbm, values, chunk_count)
-    for copy in key_copies + value_copies:
+    key_copies = copies(keys_hbm, keys, key_cuts, 0)
+    value_copies = copies(values_hbm, values, value_cuts, len(key_cuts) - 1)
+    for copy in small_copies + key_copies + value_copies:
         copy.start()
 
-    length = lengths_ref[0]
-    for copy in small_copies[:-1]:
-        copy.wait()
-    queries = queries_ref[...]
+    def side_by_side(ref, low, high):
+        return jnp.concatenate([ref[k, low:high, :] for k in range(key_heads)], axis=1)
+
     head_rows = lax.broadcasted_iota(jnp.int32, (heads, 1), 0)
-    wide = jnp.concatenate(
-        [jnp.where(head_rows // groups == k, queries, jnp.zeros_like(queries)) for k in range(key_heads)],
-        axis=1,
-    )
 
     def per_head(ref):
         rows = ref[...].astype(jnp.float32)
@@ -249,6 +247,17 @@
             total = jnp.where(head_rows // groups == k, rows[k : k + 1, :], total)
         return total
 
+    for copy in small_copies:
+        copy.wait()
+    length = lengths_ref[0]
+    queries = queries_ref[...]
+    wide = jnp.concatenate(
+        [
+            jnp.where(head_rows // groups == k, queries, jnp.zeros_like(queries))
+            for k in range(key_heads)
+        ],
+        axis=1,
+    )
     own_score = (
         jnp.sum(queries.astype(jnp.float32) * per_head(fresh_ref), axis=1, keepdims=True) * inv_root
     )
@@ -256,39 +265,35 @@
     diagonal = lax.broadcasted_iota(jnp.int32, (heads, heads), 1) == head_rows
     logit = jnp.sum(jnp.where(diagonal, logit_row, 0.0), axis=1, keepdims=True)
     log_gate = jnp.minimum(logit, 0.0) - jnp.log1p(jnp.exp(-jnp.abs(logit)))
-    small_copies[-1].wait()
     positions = lax.broadcasted_iota(jnp.int32, (heads, span), 1)
-    latest = jnp.sum(
-        jnp.where(positions == length - 1, cumlog[...], 0.0), axis=1, keepdims=True
-    )
-    offset = latest + log_gate
-    scores = []
-    for c in range(chunk_count):
-        key_copies[c].wait()
-        block = jnp.concatenate(
-            [keys[k, c * step : (c + 1) * step, :] for k in range(key_heads)], axis=1
+    cumlog = scores[...]
+    latest = jnp.sum(jnp.where(positions == length - 1, cumlog, 0.0), axis=1, keepdims=True)
+    scores[...] = jnp.where(positions < length, latest + log_gate - cumlog, -jnp.inf)
+    top = own_score
+    for copy, (low, high) in zip(key_copies, pieces(key_cuts)):
+        copy.wait()
+        raw = lax.dot_general(
+            wide,
+            side_by_side(keys, low, high),
+            contract_last,
+            preferred_element_type=jnp.float32,
         )
-        raw = lax.dot_general(wide, block, contract_last, preferred_element_type=jnp.float32)
-        raw = raw * inv_root + offset - cumlog[:, c * step : (c + 1) * step]
-        visible = positions[:, c * step : (c + 1) * step] < length
-        scores.append(jnp.where(visible, raw, -jnp.inf))
-    top = own_score
-    for part in scores:
+        part = raw * inv_root + scores[:, low:high]
+        scores[:, low:high] = part
         top = jnp.maximum(top, jnp.max(part, axis=1, keepdims=True))
+    weights = jnp.exp(scores[...] - top)
     own_weight = jnp.exp(own_score - top)
-    denominator = own_weight
+    denominator = own_weight + jnp.sum(weights, axis=1, keepdims=True)
+    weights = weights.astype(jnp.bfloat16)
+    mine = own_weight.astype(jnp.bfloat16).astype(jnp.float32) * per_head(value_new_ref)
     total = jnp.zeros((heads, key_heads * size), jnp.float32)
-    for c in range(chunk_count):
-        weights = jnp.exp(scores[c] - top)
-        denominator = denominator + jnp.sum(weights, axis=1, keepdims=True)
-        value_copies[c].wait()
-        block = jnp.concatenate(
-            [values[k, c * step : (c + 1) * step, :] for k in range(key_heads)], axis=1
+    for copy, (low, high) in zip(value_copies, pieces(value_cuts)):
+        copy.wait()
+        total = total + jnp.dot(
+            weights[:, low:high],
+            side_by_side(values, low, high),
+            preferred_element_type=jnp.float32,
         )
-        total = total + jnp.dot(
-            weights.astype(jnp.bfloat16), block, preferred_element_type=jnp.float32
-        )
-    mine = own_weight.astype(jnp.bfloat16).astype(jnp.float32) * per_head(value_new_ref)
     for k in range(key_heads):
         mine = mine + jnp.where(
             head_rows // groups == k, total[:, k * size : (k + 1) * size], 0.0
@@ -296,6 +301,42 @@
     attended = (mine / denominator).astype(jnp.bfloat16)
     for peer in range(out_ref.shape[0]):
         out_ref[peer] = attended
+
+
+def attend(queries, fresh_token_key, value_new, forget_logit, cache_keys, cache_values, cache_cumlog, lengths):
+    peers = lax.axis_size("ep")
+    _, heads, size = queries.shape
+    _, key_heads, span, _ = cache_keys.shape
+    bf16 = jnp.bfloat16
+    return pl.pallas_call(
+        attention_kernel,
+        out_shape=VMEM((peers, heads, size), bf16),
+        in_specs=[pl.BlockSpec(memory_space=pltpu.SMEM)] + [in_hbm()] * 7,
+        out_specs=in_vmem(),
+        scratch_shapes=[
+            VMEM((heads, size), bf16),
+            VMEM((key_heads, size), bf16),
+            VMEM((key_heads, size), bf16),
+            VMEM((1, heads), jnp.float32),
+            VMEM((key_heads, span, size), bf16),
+            VMEM((key_heads, span, size), bf16),
+            VMEM((heads, span), jnp.float32),
+            pltpu.SemaphoreType.DMA((len(key_cuts) + len(value_cuts) + 3,)),
+        ],
+        compiler_params=params(12),
+        name="attention",
+    )(
+        lengths,
+        *held_in_hbm(
+            queries,
+            fresh_token_key,
+            value_new,
+            forget_logit,
+            cache_keys,
+            cache_values,
+            cache_cumlog,
+        ),
+    )
 
 
 def projection_kernel(rows_ref, weight_ref, residual_ref, out_ref):
@@ -351,6 +392,9 @@
     def against(matrix):
         return lax.dot_general(matrix, normed, contract_last, preferred_element_type=jnp.float32)
 
+    hidden = (silu_product(against(gate_ref[...]), against(up_ref[...])) * share).astype(
+        jnp.bfloat16
+    )
     shared_hidden = silu_product(against(shared_gate_ref[...]), against(shared_up_ref[...])).astype(
         jnp.bfloat16
     )
@@ -363,15 +407,44 @@
     shared_rows = lax.dot_general(
         shared_hidden, spread, contract_first, preferred_element_type=jnp.float32
     ).astype(jnp.bfloat16)
-    hidden = (silu_product(against(gate_ref[...]), against(up_ref[...])) * share).astype(
-        jnp.bfloat16
-    )
     result = lax.dot_general(
         hidden, down_ref[...], contract_first, preferred_element_type=jnp.float32
     ).astype(jnp.bfloat16)
     for p in range(peers):
         out_ref[p, :tokens, :] = result[:, p * width : (p + 1) * width]
         out_ref[p, tokens:, :] = shared_rows
+
+
+def run_experts(
+    blocks,
+    norm_gain,
+    routes,
+    route_scores,
+    expert_gate,
+    expert_up,
+    expert_down,
+    shared_gate,
+    shared_up,
+):
+    peers, tokens, width = blocks.shape
+    bf16 = jnp.bfloat16
+    return pl.pallas_call(
+        expert_kernel,
+        out_shape=VMEM((peers, 2 * tokens, width), bf16),
+        in_specs=[in_vmem()] * 9,
+        out_specs=in_vmem(),
+        compiler_params=params(16),
+        name="experts",
+    )(
+        blocks,
+        norm_gain.reshape(peers, width),
+        routes.T,
+        route_scores.T,
+        *(
+            pltpu.with_memory_space_constraint(a, VMEM)
+            for a in (expert_gate[0], expert_up[0], expert_down[0], shared_gate, shared_up)
+        ),
+    )
 
 
 def combine_kernel(received_ref, stream_ref, down_ref, out_ref):
@@ -388,6 +461,19 @@
             preferred_element_type=jnp.float32,
         )
     out_ref[...] = total.astype(jnp.bfloat16)
+
+
+def combine(received, stream, shared_down):
+    tokens, width = stream.shape[1:]
+    bf16 = jnp.bfloat16
+    return pl.pallas_call(
+        combine_kernel,
+        out_shape=jax.ShapeDtypeStruct((tokens, width), bf16),
+        in_specs=[in_vmem()] * 3,
+        out_specs=in_vmem(),
+        compiler_params=params(4),
+        name="combine",
+    )(received, stream, shared_down)
 
 
 def exchange(blocks):
@@ -420,34 +506,15 @@
     _, key_heads, span, _ = cache_keys.shape
     tokens, width = residual.shape
     bf16 = jnp.bfloat16
-    spread = pl.pallas_call(
-        attention_kernel,
-        out_shape=VMEM((peers, heads, size), bf16),
-        in_specs=[pl.BlockSpec(memory_space=pltpu.SMEM)] + [in_hbm()] * 7,
-        out_specs=in_vmem(),
-        scratch_shapes=[
-            VMEM((heads, size), bf16),
-            VMEM((key_heads, size), bf16),
-            VMEM((key_heads, size), bf16),
-            VMEM((1, heads), jnp.float32),
-            VMEM((key_heads, span, size), bf16),
-            VMEM((key_heads, span, size), bf16),
-            VMEM((heads, span), jnp.float32),
-            pltpu.SemaphoreType.DMA((2 * chunk_count + 5,)),
-        ],
-        compiler_params=params(12),
-        name="attention",
-    )(
+    spread = attend(
+        queries,
+        fresh_token_key,
+        value_new,
+        forget_logit,
+        cache_keys,
+        cache_values,
+        cache_cumlog,
         lengths,
-        *held_in_hbm(
-            queries,
-            fresh_token_key,
-            value_new,
-            forget_logit,
-            cache_keys,
-            cache_values,
-            cache_cumlog,
-        ),
     )
     rows = exchange(spread)
     stream = pl.pallas_call(
@@ -460,32 +527,19 @@
         name="projection",
     )(rows, out_weight, residual)
     blocks = exchange(stream)
-    outgoing = pl.pallas_call(
-        expert_kernel,
-        out_shape=VMEM((peers, 2 * tokens, width), bf16),
-        in_specs=[in_vmem()] * 9,
-        out_specs=in_vmem(),
-        compiler_params=params(16),
-        name="experts",
-    )(
+    outgoing = run_experts(
         blocks,
-        norm_gain.reshape(peers, width),
-        routes.T,
-        route_scores.T,
-        *(
-            pltpu.with_memory_space_constraint(a, VMEM)
-            for a in (expert_gate[0], expert_up[0], expert_down[0], shared_gate, shared_up)
-        ),
+        norm_gain,
+        routes,
+        route_scores,
+        expert_gate,
+        expert_up,
+        expert_down,
+        shared_gate,
+        shared_up,
     )
     received = exchange(outgoing)
-    return pl.pallas_call(
-        combine_kernel,
-        out_shape=jax.ShapeDtypeStruct((tokens, width), bf16),
-        in_specs=[in_vmem()] * 3,
-        out_specs=in_vmem(),
-        compiler_params=params(4),
-        name="combine",
-    )(received, stream, shared_down)
+    return combine(received, stream, shared_down)
 
 
 def on_device(*arrays):
@@ -498,7 +552,7 @@
         and shared_gate.shape[0] <= residual.shape[1]
         and expert_gate.shape[0] == 1
         and queries.shape[0] == 1
-        and cache_keys.shape[2] % (128 * chunk_count) == 0
+        and cache_keys.shape[2] % 2048 == 0
     )
     return kernel_device(*arrays) if fits else plain_device(*arrays)
 

time: 42.6 us -> 42.3 us (level)
  no operation moved by 1% of the time
where the time goes in v3:
time: 42.3 us; the launch traced here: 42 us
  blocking collectives  34.4 us (81%)
  Pallas kernels  6.8 us (16%)
  between operations  0.82 us (2%)
    all_to_all x3, blocking collectives, exchange(): return lax.all_to_all(blocks, 'ep', split_axis=0, concat_axis=0, tiled=True)  34.4 us
    pallas_call x1, Pallas kernels, attend(): pl.pallas_call(attention_kernel, out_shape=VMEM((peers, heads, size), bf1...  3.29 us
    pallas_call x1, Pallas kernels, run_experts(): pl.pallas_call(expert_kernel, out_shape=VMEM((peers, 2 * tokens, width),...  2.46 us

profile of v3, /device:TPU:0, one launch (start us, length us, event | category | flops | bytes accessed | tf_op | source)
XLA Modules:
  0.0 42.0 jit_solution(6222932472278159502)
XLA Ops:
  0.0 0.0 copy-start.9
  0.0 0.0 copy-start.10
  0.7 3.3 %attention.1 = bf16[16,8,128]{2,1,0:T(8,128)(2,1)S(1)} custom-call(s32[1]{0:T(128)S(6)} %copy.20.lengths_ref, bf16[1,8,128]{2,1,0:T(8,128)(2,1)} %queries_hbm.1, bf16[1,2,128]{2,1,0:T(2,128)(2,1)} %fresh_hbm.1, bf16[1,2,128]{2,1,0:T(2,128)(2,1)} %value_new_hbm.1, f32[1,8]{1,0:T(1,128)} %forget_hbm.1, bf16[1,2,4096,128]{3,2,1,0:T(8,128)(2,1)} %keys_hbm.1, ...), custom_call_target="tpu_custom_call" | custom-call | tf_op jit(solution)/shard_map/attention/pallas_call | solution.py:311
  4.0 13.8 %all_to_all.15.rows_ref = bf16[16,8,128]{2,1,0:T(8,128)(2,1)S(1)} all-to-all(bf16[16,8,128]{2,1,0:T(8,128)(2,1)S(1)} %attention.1), channel_id=1, replica_groups=mesh['grp'=2,'ep'=16] {'ep'}, dimensions={0} | all-to-all | bytes 65536 | tf_op jit(solution)/shard_map/all_to_all | solution.py:480
  17.8 0.0 copy-done.9
  17.9 0.0 copy-done.10
  17.9 0.0 copy-start
  17.9 0.0 copy-start.1
  17.9 0.0 copy-start.2
  17.9 0.0 copy-start.3
  17.9 0.0 copy-start.4
  17.9 0.0 copy-start.6
  17.9 0.0 copy-start.7
  17.9 0.0 copy-start.8
  17.9 0.2 projection.1.stream_ref
  18.2 10.0 %all_to_all.16.blocks_ref = bf16[16,16,128]{2,1,0:T(8,128)(2,1)S(1)} all-to-all(bf16[16,16,128]{2,1,0:T(8,128)(2,1)S(1)} %projection.1.stream_ref), channel_id=1, replica_groups=mesh['grp'=2,'ep'=16] {'ep'}, dimensions={0} | all-to-all | bytes 131072 | tf_op jit(solution)/shard_map/all_to_all | solution.py:480
  28.2 0.0 copy-done
  28.2 0.0 copy-done.1
  28.2 0.0 copy-done.2
  28.2 0.0 copy-done.3
  28.2 0.0 copy-done.4
  28.2 0.0 copy-done.6
  28.2 0.0 copy-done.7
  28.2 0.0 copy-done.8
  28.2 0.0 copy-start.5
  28.3 2.5 %experts.1 = bf16[16,32,128]{2,1,0:T(8,128)(2,1)S(1)} custom-call(bf16[16,16,128]{2,1,0:T(8,128)(2,1)S(1)} %all_to_all.16.blocks_ref, f32[16,128]{1,0:T(8,128)S(1)} %bitcast.9, s32[6,16]{1,0:T(8,128)S(1)} %bitcast.10, f32[6,16]{1,0:T(8,128)S(1)} %bitcast.11, bf16[704,2048]{1,0:T(8,128)(2,1)S(1)} %bitcast.6, bf16[704,2048]{1,0:T(8,128)(2,1)S(1)} %bitcast.7, ...), custom_call_target="tpu_custom_call" | custom-call | tf_op jit(solution)/shard_map/experts/pallas_call | solution.py:431
  30.7 10.5 %all_to_all.17.received_ref = bf16[16,32,128]{2,1,0:T(8,128)(2,1)S(1)} all-to-all(bf16[16,32,128]{2,1,0:T(8,128)(2,1)S(1)} %experts.1), channel_id=1, replica_groups=mesh['grp'=2,'ep'=16] {'ep'}, dimensions={0} | all-to-all | bytes 262144 | tf_op jit(solution)/shard_map/all_to_all | solution.py:480
  41.2 0.0 copy-done.5
  41.2 0.8 %combine.1 = bf16[16,128]{1,0:T(8,128)(2,1)} custom-call(bf16[16,32,128]{2,1,0:T(8,128)(2,1)S(1)} %all_to_all.17.received_ref, bf16[16,16,128]{2,1,0:T(8,128)(2,1)S(1)} %projection.1.stream_ref, bf16[1408,128]{1,0:T(8,128)(2,1)S(1)} %copy-done.5), custom_call_target="tpu_custom_call" | custom-call | tf_op jit(solution)/shard_map/combine/pallas_call | solution.py:469
Async XLA Ops:
  0.0 17.9 %copy-start.9 = (bf16[1024,128]{1,0:T(8,128)(2,1)S(1)}, bf16[1024,128]{1,0:T(8,128)(2,1)}, u32[]{:S(2)}) copy-start(bf16[1024,128]{1,0:T(8,128)(2,1)} %weight_ref.1) | copy-start | bytes 786436
  0.0 17.9 %copy-start.10 = (bf16[16,128]{1,0:T(8,128)(2,1)S(1)}, bf16[16,128]{1,0:T(8,128)(2,1)}, u32[]{:S(2)}) copy-start(bf16[16,128]{1,0:T(8,128)(2,1)} %residual_ref.1) | copy-start | bytes 12292
  17.9 10.3 %copy-start = (bf16[1,704,2048]{2,1,0:T(8,128)(2,1)S(1)}, bf16[1,704,2048]{2,1,0:T(8,128)(2,1)}, u32[]{:S(2)}) copy-start(bf16[1,704,2048]{2,1,0:T(8,128)(2,1)} %param.30) | copy-start | bytes 8650756
  17.9 10.3 %copy-start.1 = (bf16[1,704,2048]{2,1,0:T(8,128)(2,1)S(1)}, bf16[1,704,2048]{2,1,0:T(8,128)(2,1)}, u32[]{:S(2)}) copy-start(bf16[1,704,2048]{2,1,0:T(8,128)(2,1)} %param.31) | copy-start | bytes 8650756
  17.9 10.3 %copy-start.2 = (bf16[1,704,2048]{2,1,0:T(8,128)(2,1)S(1)}, bf16[1,704,2048]{2,1,0:T(8,128)(2,1)}, u32[]{:S(2)}) copy-start(bf16[1,704,2048]{2,1,0:T(8,128)(2,1)} %param.32) | copy-start | bytes 8650756
  17.9 10.3 %copy-start.3 = (bf16[88,2048]{1,0:T(8,128)(2,1)S(1)}, bf16[88,2048]{1,0:T(8,128)(2,1)}, u32[]{:S(2)}) copy-start(bf16[88,2048]{1,0:T(8,128)(2,1)} %shared_gate_ref.1) | copy-start | bytes 1081348
  17.9 10.3 %copy-start.4 = (bf16[88,2048]{1,0:T(8,128)(2,1)S(1)}, bf16[88,2048]{1,0:T(8,128)(2,1)}, u32[]{:S(2)}) copy-start(bf16[88,2048]{1,0:T(8,128)(2,1)} %shared_up_ref.1) | copy-start | bytes 1081348
  17.9 10.3 %copy-start.6 = (f32[2048]{0:T(1024)S(1)}, f32[2048]{0:T(1024)}, u32[]{:S(2)}) copy-start(f32[2048]{0:T(1024)} %param.29) | copy-start | bytes 24580
  17.9 10.3 %copy-start.7 = (s32[16,6]{0,1:T(8,128)S(1)}, s32[16,6]{0,1:T(8,128)}, u32[]{:S(2)}) copy-start(s32[16,6]{0,1:T(8,128)} %param.36) | copy-start | bytes 1156
  17.9 10.3 %copy-start.8 = (f32[16,6]{0,1:T(8,128)S(1)}, f32[16,6]{0,1:T(8,128)}, u32[]{:S(2)}) copy-start(f32[16,6]{0,1:T(8,128)} %param.37) | copy-start | bytes 1156
  28.2 13.0 %copy-start.5 = (bf16[1408,128]{1,0:T(8,128)(2,1)S(1)}, bf16[1408,128]{1,0:T(8,128)(2,1)}, u32[]{:S(2)}) copy-start(bf16[1408,128]{1,0:T(8,128)(2,1)} %down_ref.1) | copy-start | bytes 1081348

commit v4 on v3

--- a/solution.py
+++ b/solution.py
@@ -159,8 +159,8 @@
 
 
 VMEM = pltpu.VMEM
-key_cuts = (0, 1, 4)
-value_cuts = (0, 4)
+cuts = (0, 1, 4, 8)
+ahead = 2
 
 
 def in_vmem():
@@ -202,7 +202,7 @@
     key_heads, span, _ = keys.shape
     groups = heads // key_heads
     inv_root = size ** (-0.5)
-    first = len(key_cuts) + len(value_cuts) - 2
+    first = 2 * len(cuts) - 2
     small_copies = [
         pltpu.make_async_copy(source, target, sems.at[first + i])
         for i, (source, target) in enumerate(
@@ -230,8 +230,8 @@
             for i, (low, high) in enumerate(pieces(cuts))
         ]
 
-    key_copies = copies(keys_hbm, keys, key_cuts, 0)
-    value_copies = copies(values_hbm, values, value_cuts, len(key_cuts) - 1)
+    key_copies = copies(keys_hbm, keys, cuts, 0)
+    value_copies = copies(values_hbm, values, cuts, len(cuts) - 1)
     for copy in small_copies + key_copies + value_copies:
         copy.start()
 
@@ -269,31 +269,48 @@
     cumlog = scores[...]
     latest = jnp.sum(jnp.where(positions == length - 1, cumlog, 0.0), axis=1, keepdims=True)
     scores[...] = jnp.where(positions < length, latest + log_gate - cumlog, -jnp.inf)
-    top = own_score
-    for copy, (low, high) in zip(key_copies, pieces(key_cuts)):
-        copy.wait()
+    parts = pieces(cuts)
+
+    def score(i):
+        low, high = parts[i]
         raw = lax.dot_general(
             wide,
             side_by_side(keys, low, high),
             contract_last,
             preferred_element_type=jnp.float32,
         )
-        part = raw * inv_root + scores[:, low:high]
-        scores[:, low:high] = part
-        top = jnp.maximum(top, jnp.max(part, axis=1, keepdims=True))
-    weights = jnp.exp(scores[...] - top)
+        return raw * inv_root + scores[:, low:high]
+
+    def attend_to(weights, i):
+        low, high = parts[i]
+        return jnp.dot(weights, side_by_side(values, low, high), preferred_element_type=jnp.float32)
+
+    count = len(parts)
+    ready = [None] * count
+    def fold(state, i):
+        top, total, denominator = state
+        new_top = jnp.maximum(top, jnp.max(ready[i], axis=1, keepdims=True))
+        weights = jnp.exp(ready[i] - new_top)
+        added = jnp.sum(weights, axis=1, keepdims=True)
+        value_copies[i].wait()
+        product = attend_to(weights.astype(jnp.bfloat16), i)
+        if total is None:
+            return new_top, product, added
+        shrink = jnp.exp(top - new_top)
+        return new_top, total * shrink + product, denominator * shrink + added
+
+    state = own_score, None, None
+    for i in range(count):
+        key_copies[i].wait()
+        ready[i] = score(i)
+        if i >= ahead:
+            state = fold(state, i - ahead)
+    for i in range(max(count - ahead, 0), count):
+        state = fold(state, i)
+    top, total, denominator = state
     own_weight = jnp.exp(own_score - top)
-    denominator = own_weight + jnp.sum(weights, axis=1, keepdims=True)
-    weights = weights.astype(jnp.bfloat16)
+    denominator = denominator + own_weight
     mine = own_weight.astype(jnp.bfloat16).astype(jnp.float32) * per_head(value_new_ref)
-    total = jnp.zeros((heads, key_heads * size), jnp.float32)
-    for copy, (low, high) in zip(value_copies, pieces(value_cuts)):
-        copy.wait()
-        total = total + jnp.dot(
-            weights[:, low:high],
-            side_by_side(values, low, high),
-            preferred_element_type=jnp.float32,
-        )
     for k in range(key_heads):
         mine = mine + jnp.where(
             head_rows // groups == k, total[:, k * size : (k + 1) * size], 0.0
@@ -321,7 +338,7 @@
             VMEM((key_heads, span, size), bf16),
             VMEM((key_heads, span, size), bf16),
             VMEM((heads, span), jnp.float32),
-            pltpu.SemaphoreType.DMA((len(key_cuts) + len(value_cuts) + 3,)),
+            pltpu.SemaphoreType.DMA((2 * len(cuts) + 3,)),
         ],
         compiler_params=params(12),
         name="attention",
@@ -392,23 +409,21 @@
     def against(matrix):
         return lax.dot_general(matrix, normed, contract_last, preferred_element_type=jnp.float32)
 
-    hidden = (silu_product(against(gate_ref[...]), against(up_ref[...])) * share).astype(
-        jnp.bfloat16
-    )
-    shared_hidden = silu_product(against(shared_gate_ref[...]), against(shared_up_ref[...])).astype(
-        jnp.bfloat16
-    )
-    units = shared_hidden.shape[0]
+    units = shared_gate_ref.shape[0]
     spread = (
         lax.broadcasted_iota(jnp.int32, (units, width), 0)
         == lax.broadcasted_iota(jnp.int32, (units, width), 1)
     ).astype(jnp.bfloat16)
     contract_first = (((0,), (0,)), ((), ()))
+    halves = (against(gate_ref[...]), against(up_ref[...]))
+    shared_halves = (against(shared_gate_ref[...]), against(shared_up_ref[...]))
+    hidden = (silu_product(*halves) * share).astype(jnp.bfloat16)
+    result = lax.dot_general(
+        hidden, down_ref[...], contract_first, preferred_element_type=jnp.float32
+    ).astype(jnp.bfloat16)
+    shared_hidden = silu_product(*shared_halves).astype(jnp.bfloat16)
     shared_rows = lax.dot_general(
         shared_hidden, spread, contract_first, preferred_element_type=jnp.float32
-    ).astype(jnp.bfloat16)
-    result = lax.dot_general(
-        hidden, down_ref[...], contract_first, preferred_element_type=jnp.float32
     ).astype(jnp.bfloat16)
     for p in range(peers):
         out_ref[p, :tokens, :] = result[:, p * width : (p + 1) * width]

time: 42.3 us -> 41.7 us (0.986)
  Pallas kernels: 6.8 us -> 6.19 us
    pallas_call x1, Pallas kernels: 3.29 us -> 2.86 us  [attend(): pl.pallas_call(attention_kernel, out_shape=VMEM((peers, heads, size), bf1...]
where the time goes in v4:
time: 41.7 us; the launch traced here: 41.4 us
  blocking collectives  34.3 us (82%)
  Pallas kernels  6.19 us (15%)
  between operations  0.83 us (2%)
    all_to_all x3, blocking collectives, exchange(): return lax.all_to_all(blocks, 'ep', split_axis=0, concat_axis=0, tiled=True)  34.3 us
    pallas_call x1, Pallas kernels, attend(): pl.pallas_call(attention_kernel, out_shape=VMEM((peers, heads, size), bf1...  2.86 us
    pallas_call x1, Pallas kernels, run_experts(): pl.pallas_call(expert_kernel, out_shape=VMEM((peers, 2 * tokens, width),...  2.28 us

profile of v4, /device:TPU:0, one launch (start us, length us, event | category | flops | bytes accessed | tf_op | source)
XLA Modules:
  0.0 41.4 jit_solution(14231459949336597762)
XLA Ops:
  0.0 0.0 copy-start.9
  0.0 0.0 copy-start.10
  0.7 2.9 %attention.1 = bf16[16,8,128]{2,1,0:T(8,128)(2,1)S(1)} custom-call(s32[1]{0:T(128)S(6)} %copy.20.lengths_ref, bf16[1,8,128]{2,1,0:T(8,128)(2,1)} %queries_hbm.1, bf16[1,2,128]{2,1,0:T(2,128)(2,1)} %fresh_hbm.1, bf16[1,2,128]{2,1,0:T(2,128)(2,1)} %value_new_hbm.1, f32[1,8]{1,0:T(1,128)} %forget_hbm.1, bf16[1,2,4096,128]{3,2,1,0:T(8,128)(2,1)} %keys_hbm.1, ...), custom_call_target="tpu_custom_call" | custom-call | tf_op jit(solution)/shard_map/attention/pallas_call | solution.py:328
  3.6 13.8 %all_to_all.15.rows_ref = bf16[16,8,128]{2,1,0:T(8,128)(2,1)S(1)} all-to-all(bf16[16,8,128]{2,1,0:T(8,128)(2,1)S(1)} %attention.1), channel_id=1, replica_groups=mesh['grp'=2,'ep'=16] {'ep'}, dimensions={0} | all-to-all | bytes 65536 | tf_op jit(solution)/shard_map/all_to_all | solution.py:495
  17.4 0.0 copy-done.9
  17.4 0.0 copy-done.10
  17.4 0.0 copy-start
  17.4 0.0 copy-start.1
  17.4 0.0 copy-start.2
  17.4 0.0 copy-start.3
  17.5 0.0 copy-start.4
  17.5 0.0 copy-start.6
  17.5 0.0 copy-start.7
  17.5 0.0 copy-start.8
  17.5 0.2 projection.1.stream_ref
  17.7 10.0 %all_to_all.16.blocks_ref = bf16[16,16,128]{2,1,0:T(8,128)(2,1)S(1)} all-to-all(bf16[16,16,128]{2,1,0:T(8,128)(2,1)S(1)} %projection.1.stream_ref), channel_id=1, replica_groups=mesh['grp'=2,'ep'=16] {'ep'}, dimensions={0} | all-to-all | bytes 131072 | tf_op jit(solution)/shard_map/all_to_all | solution.py:495
  27.7 0.0 copy-done
  27.8 0.0 copy-done.1
  27.8 0.0 copy-done.2
  27.8 0.0 copy-done.3
  27.8 0.0 copy-done.4
  27.8 0.0 copy-done.6
  27.8 0.0 copy-done.7
  27.8 0.0 copy-done.8
  27.8 0.0 copy-start.5
  27.8 2.3 %experts.1 = bf16[16,32,128]{2,1,0:T(8,128)(2,1)S(1)} custom-call(bf16[16,16,128]{2,1,0:T(8,128)(2,1)S(1)} %all_to_all.16.blocks_ref, f32[16,128]{1,0:T(8,128)S(1)} %bitcast.9, s32[6,16]{1,0:T(8,128)S(1)} %bitcast.10, f32[6,16]{1,0:T(8,128)S(1)} %bitcast.11, bf16[704,2048]{1,0:T(8,128)(2,1)S(1)} %bitcast.6, bf16[704,2048]{1,0:T(8,128)(2,1)S(1)} %bitcast.7, ...), custom_call_target="tpu_custom_call" | custom-call | tf_op jit(solution)/shard_map/experts/pallas_call | solution.py:446
  30.1 10.5 %all_to_all.17.received_ref = bf16[16,32,128]{2,1,0:T(8,128)(2,1)S(1)} all-to-all(bf16[16,32,128]{2,1,0:T(8,128)(2,1)S(1)} %experts.1), channel_id=1, replica_groups=mesh['grp'=2,'ep'=16] {'ep'}, dimensions={0} | all-to-all | bytes 262144 | tf_op jit(solution)/shard_map/all_to_all | solution.py:495
  40.6 0.0 copy-done.5
  40.6 0.8 %combine.1 = bf16[16,128]{1,0:T(8,128)(2,1)} custom-call(bf16[16,32,128]{2,1,0:T(8,128)(2,1)S(1)} %all_to_all.17.received_ref, bf16[16,16,128]{2,1,0:T(8,128)(2,1)S(1)} %projection.1.stream_ref, bf16[1408,128]{1,0:T(8,128)(2,1)S(1)} %copy-done.5), custom_call_target="tpu_custom_call" | custom-call | tf_op jit(solution)/shard_map/combine/pallas_call | solution.py:484
Async XLA Ops:
  0.0 17.4 %copy-start.9 = (bf16[1024,128]{1,0:T(8,128)(2,1)S(1)}, bf16[1024,128]{1,0:T(8,128)(2,1)}, u32[]{:S(2)}) copy-start(bf16[1024,128]{1,0:T(8,128)(2,1)} %weight_ref.1) | copy-start | bytes 786436
  0.0 17.4 %copy-start.10 = (bf16[16,128]{1,0:T(8,128)(2,1)S(1)}, bf16[16,128]{1,0:T(8,128)(2,1)}, u32[]{:S(2)}) copy-start(bf16[16,128]{1,0:T(8,128)(2,1)} %residual_ref.1) | copy-start | bytes 12292
  17.4 10.3 %copy-start = (bf16[1,704,2048]{2,1,0:T(8,128)(2,1)S(1)}, bf16[1,704,2048]{2,1,0:T(8,128)(2,1)}, u32[]{:S(2)}) copy-start(bf16[1,704,2048]{2,1,0:T(8,128)(2,1)} %param.30) | copy-start | bytes 8650756
  17.4 10.3 %copy-start.1 = (bf16[1,704,2048]{2,1,0:T(8,128)(2,1)S(1)}, bf16[1,704,2048]{2,1,0:T(8,128)(2,1)}, u32[]{:S(2)}) copy-start(bf16[1,704,2048]{2,1,0:T(8,128)(2,1)} %param.31) | copy-start | bytes 8650756
  17.4 10.3 %copy-start.2 = (bf16[1,704,2048]{2,1,0:T(8,128)(2,1)S(1)}, bf16[1,704,2048]{2,1,0:T(8,128)(2,1)}, u32[]{:S(2)}) copy-start(bf16[1,704,2048]{2,1,0:T(8,128)(2,1)} %param.32) | copy-start | bytes 8650756
  17.4 10.3 %copy-start.3 = (bf16[88,2048]{1,0:T(8,128)(2,1)S(1)}, bf16[88,2048]{1,0:T(8,128)(2,1)}, u32[]{:S(2)}) copy-start(bf16[88,2048]{1,0:T(8,128)(2,1)} %shared_gate_ref.1) | copy-start | bytes 1081348
  17.5 10.3 %copy-start.4 = (bf16[88,2048]{1,0:T(8,128)(2,1)S(1)}, bf16[88,2048]{1,0:T(8,128)(2,1)}, u32[]{:S(2)}) copy-start(bf16[88,2048]{1,0:T(8,128)(2,1)} %shared_up_ref.1) | copy-start | bytes 1081348
  17.5 10.3 %copy-start.6 = (f32[2048]{0:T(1024)S(1)}, f32[2048]{0:T(1024)}, u32[]{:S(2)}) copy-start(f32[2048]{0:T(1024)} %param.29) | copy-start | bytes 24580
  17.5 10.3 %copy-start.7 = (s32[16,6]{0,1:T(8,128)S(1)}, s32[16,6]{0,1:T(8,128)}, u32[]{:S(2)}) copy-start(s32[16,6]{0,1:T(8,128)} %param.36) | copy-start | bytes 1156
  17.5 10.3 %copy-start.8 = (f32[16,6]{0,1:T(8,128)S(1)}, f32[16,6]{0,1:T(8,128)}, u32[]{:S(2)}) copy-start(f32[16,6]{0,1:T(8,128)} %param.37) | copy-start | bytes 1156
  27.8 12.8 %copy-start.5 = (bf16[1408,128]{1,0:T(8,128)(2,1)S(1)}, bf16[1408,128]{1,0:T(8,128)(2,1)}, u32[]{:S(2)}) copy-start(bf16[1408,128]{1,0:T(8,128)(2,1)} %down_ref.1) | copy-start | bytes 1081348

commit v5 on v4

--- a/solution.py
+++ b/solution.py
@@ -287,6 +287,7 @@
 
     count = len(parts)
     ready = [None] * count
+
     def fold(state, i):
         top, total, denominator = state
         new_top = jnp.maximum(top, jnp.max(ready[i], axis=1, keepdims=True))
@@ -316,8 +317,12 @@
             head_rows // groups == k, total[:, k * size : (k + 1) * size], 0.0
         )
     attended = (mine / denominator).astype(jnp.bfloat16)
+    out_ref[...] = attended
+
+
+def spread_kernel(own_ref, out_ref):
     for peer in range(out_ref.shape[0]):
-        out_ref[peer] = attended
+        out_ref[peer] = own_ref[...]
 
 
 def attend(queries, fresh_token_key, value_new, forget_logit, cache_keys, cache_values, cache_cumlog, lengths):
@@ -325,9 +330,9 @@
     _, heads, size = queries.shape
     _, key_heads, span, _ = cache_keys.shape
     bf16 = jnp.bfloat16
-    return pl.pallas_call(
+    own = pl.pallas_call(
         attention_kernel,
-        out_shape=VMEM((peers, heads, size), bf16),
+        out_shape=VMEM((heads, size), bf16),
         in_specs=[pl.BlockSpec(memory_space=pltpu.SMEM)] + [in_hbm()] * 7,
         out_specs=in_vmem(),
         scratch_shapes=[
@@ -354,6 +359,17 @@
             cache_cumlog,
         ),
     )
+    return pl.pallas_call(
+        spread_kernel,
+        out_shape=VMEM((peers, heads, size), bf16),
+        in_specs=[in_vmem()],
+        out_specs=in_vmem(),
+        compiler_params=params(4),
+        cost_estimate=pl.CostEstimate(
+            flops=100000000000, bytes_accessed=0, transcendentals=0
+        ),
+        name="spread",
+    )(own)
 
 
 def projection_kernel(rows_ref, weight_ref, residual_ref, out_ref):
@@ -538,7 +554,6 @@
         in_specs=[in_vmem()] * 3,
         out_specs=in_vmem(),
         compiler_params=params(4),
-        cost_estimate=pl.CostEstimate(flops=100000000000, bytes_accessed=0, transcendentals=0),
         name="projection",
     )(rows, out_weight, residual)
     blocks = exchange(stream)

time: 41.7 us -> 41.4 us (level)
    pallas_call x1 -> x2, Pallas kernels: 2.86 us -> 2.87 us  [the longest x1 2.86 us: attend(): pl.pallas_call(attention_kernel, out_shape=VMEM((heads, size), bf16), in_...]
where the time goes in v5:
time: 41.4 us; the launch traced here: 41.2 us
  blocking collectives  34.1 us (82%)
  Pallas kernels  6.2 us (15%)
  between operations  0.82 us (2%)
    all_to_all x3, blocking collectives, exchange(): return lax.all_to_all(blocks, 'ep', split_axis=0, concat_axis=0, tiled=True)  34.1 us
    pallas_call x1, Pallas kernels, attend(): pl.pallas_call(attention_kernel, out_shape=VMEM((heads, size), bf16), in_...  2.86 us
    pallas_call x1, Pallas kernels, run_experts(): pl.pallas_call(expert_kernel, out_shape=VMEM((peers, 2 * tokens, width),...  2.28 us

profile of v5, /device:TPU:0, one launch (start us, length us, event | category | flops | bytes accessed | tf_op | source)
XLA Modules:
  0.0 41.2 jit_solution(1686573898178966768)
XLA Ops:
  0.7 2.9 %attention.1.own_ref = bf16[8,128]{1,0:T(8,128)(2,1)S(1)} custom-call(s32[1]{0:T(128)S(6)} %copy.20.lengths_ref, bf16[1,8,128]{2,1,0:T(8,128)(2,1)} %queries_hbm.1, bf16[1,2,128]{2,1,0:T(2,128)(2,1)} %fresh_hbm.1, bf16[1,2,128]{2,1,0:T(2,128)(2,1)} %value_new_hbm.1, f32[1,8]{1,0:T(1,128)} %forget_hbm.1, bf16[1,2,4096,128]{3,2,1,0:T(8,128)(2,1)} %keys_hbm.1, ...), custom_call_target="tpu_custom_call" | custom-call | tf_op jit(solution)/shard_map/attention/pallas_call | solution.py:333
  3.5 0.0 copy-start.6
  3.5 0.0 copy-start.8
  3.5 0.0 copy-start
  3.6 0.0 copy-start.1
  3.6 0.0 copy-start.2
  3.6 0.0 copy-start.3
  3.6 0.0 copy-start.4
  3.6 0.0 copy-start.7
  3.6 0.0 copy-start.9
  3.6 0.0 copy-start.10
  3.7 14.1 %all_to_all.15.rows_ref = bf16[16,8,128]{2,1,0:T(8,128)(2,1)S(1)} all-to-all(bf16[16,8,128]{2,1,0:T(8,128)(2,1)S(1)} %spread.1), channel_id=1, replica_groups=mesh['grp'=2,'ep'=16] {'ep'}, dimensions={0} | all-to-all | bytes 65536 | tf_op jit(solution)/shard_map/all_to_all | solution.py:511
  17.8 0.0 copy-done.6
  17.8 0.0 copy-done.8
  17.8 0.2 projection.1.stream_ref
  18.0 9.5 %all_to_all.16.blocks_ref = bf16[16,16,128]{2,1,0:T(8,128)(2,1)S(1)} all-to-all(bf16[16,16,128]{2,1,0:T(8,128)(2,1)S(1)} %projection.1.stream_ref), channel_id=1, replica_groups=mesh['grp'=2,'ep'=16] {'ep'}, dimensions={0} | all-to-all | bytes 131072 | tf_op jit(solution)/shard_map/all_to_all | solution.py:511
  27.5 0.0 copy-done
  27.5 0.0 copy-done.1
  27.5 0.0 copy-done.2
  27.5 0.0 copy-done.3
  27.5 0.0 copy-done.4
  27.5 0.0 copy-done.7
  27.5 0.0 copy-done.9
  27.5 0.0 copy-done.10
  27.6 0.0 copy-start.5
  27.6 2.3 %experts.1 = bf16[16,32,128]{2,1,0:T(8,128)(2,1)S(1)} custom-call(bf16[16,16,128]{2,1,0:T(8,128)(2,1)S(1)} %all_to_all.16.blocks_ref, f32[16,128]{1,0:T(8,128)S(1)} %bitcast.9, s32[6,16]{1,0:T(8,128)S(1)} %bitcast.10, f32[6,16]{1,0:T(8,128)S(1)} %bitcast.11, bf16[704,2048]{1,0:T(8,128)(2,1)S(1)} %bitcast.6, bf16[704,2048]{1,0:T(8,128)(2,1)S(1)} %bitcast.7, ...), custom_call_target="tpu_custom_call" | custom-call | tf_op jit(solution)/shard_map/experts/pallas_call | solution.py:462
  29.9 10.5 %all_to_all.17.received_ref = bf16[16,32,128]{2,1,0:T(8,128)(2,1)S(1)} all-to-all(bf16[16,32,128]{2,1,0:T(8,128)(2,1)S(1)} %experts.1), channel_id=1, replica_groups=mesh['grp'=2,'ep'=16] {'ep'}, dimensions={0} | all-to-all | bytes 262144 | tf_op jit(solution)/shard_map/all_to_all | solution.py:511
  40.4 0.0 copy-done.5
  40.4 0.8 %combine.1 = bf16[16,128]{1,0:T(8,128)(2,1)} custom-call(bf16[16,32,128]{2,1,0:T(8,128)(2,1)S(1)} %all_to_all.17.received_ref, bf16[16,16,128]{2,1,0:T(8,128)(2,1)S(1)} %projection.1.stream_ref, bf16[1408,128]{1,0:T(8,128)(2,1)S(1)} %copy-done.5), custom_call_target="tpu_custom_call" | custom-call | tf_op jit(solution)/shard_map/combine/pallas_call | solution.py:500
  (1 shorter events, 0.0 us)
Async XLA Ops:
  3.5 14.2 %copy-start.6 = (bf16[1024,128]{1,0:T(8,128)(2,1)S(1)}, bf16[1024,128]{1,0:T(8,128)(2,1)}, u32[]{:S(2)}) copy-start(bf16[1024,128]{1,0:T(8,128)(2,1)} %weight_ref.1) | copy-start | bytes 786436
  3.5 14.2 %copy-start.8 = (bf16[16,128]{1,0:T(8,128)(2,1)S(1)}, bf16[16,128]{1,0:T(8,128)(2,1)}, u32[]{:S(2)}) copy-start(bf16[16,128]{1,0:T(8,128)(2,1)} %residual_ref.1) | copy-start | bytes 12292
  3.5 23.9 %copy-start = (bf16[1,704,2048]{2,1,0:T(8,128)(2,1)S(1)}, bf16[1,704,2048]{2,1,0:T(8,128)(2,1)}, u32[]{:S(2)}) copy-start(bf16[1,704,2048]{2,1,0:T(8,128)(2,1)} %param.30) | copy-start | bytes 8650756
  3.6 23.9 %copy-start.1 = (bf16[1,704,2048]{2,1,0:T(8,128)(2,1)S(1)}, bf16[1,704,2048]{2,1,0:T(8,128)(2,1)}, u32[]{:S(2)}) copy-start(bf16[1,704,2048]{2,1,0:T(8,128)(2,1)} %param.31) | copy-start | bytes 8650756
  3.6 23.9 %copy-start.2 = (bf16[1,704,2048]{2,1,0:T(8,128)(2,1)S(1)}, bf16[1,704,2048]{2,1,0:T(8,128)(2,1)}, u32[]{:S(2)}) copy-start(bf16[1,704,2048]{2,1,0:T(8,128)(2,1)} %param.32) | copy-start | bytes 8650756
  3.6 23.9 %copy-start.3 = (bf16[88,2048]{1,0:T(8,128)(2,1)S(1)}, bf16[88,2048]{1,0:T(8,128)(2,1)}, u32[]{:S(2)}) copy-start(bf16[88,2048]{1,0:T(8,128)(2,1)} %shared_gate_ref.1) | copy-start | bytes 1081348
  3.6 23.9 %copy-start.4 = (bf16[88,2048]{1,0:T(8,128)(2,1)S(1)}, bf16[88,2048]{1,0:T(8,128)(2,1)}, u32[]{:S(2)}) copy-start(bf16[88,2048]{1,0:T(8,128)(2,1)} %shared_up_ref.1) | copy-start | bytes 1081348
  3.6 23.9 %copy-start.7 = (f32[2048]{0:T(1024)S(1)}, f32[2048]{0:T(1024)}, u32[]{:S(2)}) copy-start(f32[2048]{0:T(1024)} %param.29) | copy-start | bytes 24580
  3.6 23.9 %copy-start.9 = (s32[16,6]{0,1:T(8,128)S(1)}, s32[16,6]{0,1:T(8,128)}, u32[]{:S(2)}) copy-start(s32[16,6]{0,1:T(8,128)} %param.36) | copy-start | bytes 1156
  3.6 23.9 %copy-start.10 = (f32[16,6]{0,1:T(8,128)S(1)}, f32[16,6]{0,1:T(8,128)}, u32[]{:S(2)}) copy-start(f32[16,6]{0,1:T(8,128)} %param.37) | copy-start | bytes 1156
  27.6 12.8 %copy-start.5 = (bf16[1408,128]{1,0:T(8,128)(2,1)S(1)}, bf16[1408,128]{1,0:T(8,128)(2,1)}, u32[]{:S(2)}) copy-start(bf16[1408,128]{1,0:T(8,128)(2,1)} %down_ref.1) | copy-start | bytes 1081348

commit v6 on v5

--- a/solution.py
+++ b/solution.py
@@ -554,6 +554,9 @@
         in_specs=[in_vmem()] * 3,
         out_specs=in_vmem(),
         compiler_params=params(4),
+        cost_estimate=pl.CostEstimate(
+            flops=2000000000, bytes_accessed=0, transcendentals=0
+        ),
         name="projection",
     )(rows, out_weight, residual)
     blocks = exchange(stream)

time: 41.4 us -> 41.8 us (level)
  no operation moved by 1% of the time
where the time goes in v6:
time: 41.8 us; the launch traced here: 41.5 us
  blocking collectives  34.5 us (83%)
  Pallas kernels  6.2 us (15%)
  between operations  0.81 us (2%)
    all_to_all x3, blocking collectives, exchange(): return lax.all_to_all(blocks, 'ep', split_axis=0, concat_axis=0, tiled=True)  34.5 us
    pallas_call x1, Pallas kernels, attend(): pl.pallas_call(attention_kernel, out_shape=VMEM((heads, size), bf16), in_...  2.86 us
    pallas_call x1, Pallas kernels, run_experts(): pl.pallas_call(expert_kernel, out_shape=VMEM((peers, 2 * tokens, width),...  2.28 us

profile of v6, /device:TPU:0, one launch (start us, length us, event | category | flops | bytes accessed | tf_op | source)
XLA Modules:
  0.0 41.5 jit_solution(18316330496025795459)
XLA Ops:
  0.7 2.9 %attention.1.own_ref = bf16[8,128]{1,0:T(8,128)(2,1)S(1)} custom-call(s32[1]{0:T(128)S(6)} %copy.20.lengths_ref, bf16[1,8,128]{2,1,0:T(8,128)(2,1)} %queries_hbm.1, bf16[1,2,128]{2,1,0:T(2,128)(2,1)} %fresh_hbm.1, bf16[1,2,128]{2,1,0:T(2,128)(2,1)} %value_new_hbm.1, f32[1,8]{1,0:T(1,128)} %forget_hbm.1, bf16[1,2,4096,128]{3,2,1,0:T(8,128)(2,1)} %keys_hbm.1, ...), custom_call_target="tpu_custom_call" | custom-call | tf_op jit(solution)/shard_map/attention/pallas_call | solution.py:333
  3.5 0.0 copy-start.9
  3.5 0.0 copy-start.10
  3.5 0.0 copy-start.2
  3.6 14.1 %all_to_all.15.rows_ref = bf16[16,8,128]{2,1,0:T(8,128)(2,1)S(1)} all-to-all(bf16[16,8,128]{2,1,0:T(8,128)(2,1)S(1)} %spread.1), channel_id=1, replica_groups=mesh['grp'=2,'ep'=16] {'ep'}, dimensions={0} | all-to-all | bytes 65536 | tf_op jit(solution)/shard_map/all_to_all | solution.py:511
  17.7 0.0 copy-done.9
  17.7 0.0 copy-done.10
  17.7 0.0 copy-start
  17.7 0.0 copy-start.1
  17.7 0.0 copy-start.3
  17.7 0.0 copy-start.4
  17.7 0.0 copy-start.6
  17.7 0.0 copy-start.7
  17.7 0.0 copy-start.8
  17.8 0.2 projection.1.stream_ref
  18.0 9.9 %all_to_all.16.blocks_ref = bf16[16,16,128]{2,1,0:T(8,128)(2,1)S(1)} all-to-all(bf16[16,16,128]{2,1,0:T(8,128)(2,1)S(1)} %projection.1.stream_ref), channel_id=1, replica_groups=mesh['grp'=2,'ep'=16] {'ep'}, dimensions={0} | all-to-all | bytes 131072 | tf_op jit(solution)/shard_map/all_to_all | solution.py:511
  27.9 0.0 copy-done.2
  27.9 0.0 copy-done
  27.9 0.0 copy-done.1
  27.9 0.0 copy-done.3
  27.9 0.0 copy-done.4
  27.9 0.0 copy-done.6
  27.9 0.0 copy-done.7
  27.9 0.0 copy-done.8
  27.9 0.0 copy-start.5
  27.9 2.3 %experts.1 = bf16[16,32,128]{2,1,0:T(8,128)(2,1)S(1)} custom-call(bf16[16,16,128]{2,1,0:T(8,128)(2,1)S(1)} %all_to_all.16.blocks_ref, f32[16,128]{1,0:T(8,128)S(1)} %bitcast.9, s32[6,16]{1,0:T(8,128)S(1)} %bitcast.10, f32[6,16]{1,0:T(8,128)S(1)} %bitcast.11, bf16[704,2048]{1,0:T(8,128)(2,1)S(1)} %bitcast.6, bf16[704,2048]{1,0:T(8,128)(2,1)S(1)} %bitcast.7, ...), custom_call_target="tpu_custom_call" | custom-call | tf_op jit(solution)/shard_map/experts/pallas_call | solution.py:462
  30.2 10.5 %all_to_all.17.received_ref = bf16[16,32,128]{2,1,0:T(8,128)(2,1)S(1)} all-to-all(bf16[16,32,128]{2,1,0:T(8,128)(2,1)S(1)} %experts.1), channel_id=1, replica_groups=mesh['grp'=2,'ep'=16] {'ep'}, dimensions={0} | all-to-all | bytes 262144 | tf_op jit(solution)/shard_map/all_to_all | solution.py:511
  40.7 0.0 copy-done.5
  40.7 0.8 %combine.1 = bf16[16,128]{1,0:T(8,128)(2,1)} custom-call(bf16[16,32,128]{2,1,0:T(8,128)(2,1)S(1)} %all_to_all.17.received_ref, bf16[16,16,128]{2,1,0:T(8,128)(2,1)S(1)} %projection.1.stream_ref, bf16[1408,128]{1,0:T(8,128)(2,1)S(1)} %copy-done.5), custom_call_target="tpu_custom_call" | custom-call | tf_op jit(solution)/shard_map/combine/pallas_call | solution.py:500
  (1 shorter events, 0.0 us)
Async XLA Ops:
  3.5 14.2 %copy-start.9 = (bf16[1024,128]{1,0:T(8,128)(2,1)S(1)}, bf16[1024,128]{1,0:T(8,128)(2,1)}, u32[]{:S(2)}) copy-start(bf16[1024,128]{1,0:T(8,128)(2,1)} %weight_ref.1) | copy-start | bytes 786436
  3.5 14.2 %copy-start.10 = (bf16[16,128]{1,0:T(8,128)(2,1)S(1)}, bf16[16,128]{1,0:T(8,128)(2,1)}, u32[]{:S(2)}) copy-start(bf16[16,128]{1,0:T(8,128)(2,1)} %residual_ref.1) | copy-start | bytes 12292
  3.5 24.3 %copy-start.2 = (bf16[1,704,2048]{2,1,0:T(8,128)(2,1)S(1)}, bf16[1,704,2048]{2,1,0:T(8,128)(2,1)}, u32[]{:S(2)}) copy-start(bf16[1,704,2048]{2,1,0:T(8,128)(2,1)} %param.32) | copy-start | bytes 8650756
  17.7 10.2 %copy-start = (bf16[1,704,2048]{2,1,0:T(8,128)(2,1)S(1)}, bf16[1,704,2048]{2,1,0:T(8,128)(2,1)}, u32[]{:S(2)}) copy-start(bf16[1,704,2048]{2,1,0:T(8,128)(2,1)} %param.30) | copy-start | bytes 8650756
  17.7 10.2 %copy-start.1 = (bf16[1,704,2048]{2,1,0:T(8,128)(2,1)S(1)}, bf16[1,704,2048]{2,1,0:T(8,128)(2,1)}, u32[]{:S(2)}) copy-start(bf16[1,704,2048]{2,1,0:T(8,128)(2,1)} %param.31) | copy-start | bytes 8650756
  17.7 10.2 %copy-start.3 = (bf16[88,2048]{1,0:T(8,128)(2,1)S(1)}, bf16[88,2048]{1,0:T(8,128)(2,1)}, u32[]{:S(2)}) copy-start(bf16[88,2048]{1,0:T(8,128)(2,1)} %shared_gate_ref.1) | copy-start | bytes 1081348
  17.7 10.2 %copy-start.4 = (bf16[88,2048]{1,0:T(8,128)(2,1)S(1)}, bf16[88,2048]{1,0:T(8,128)(2,1)}, u32[]{:S(2)}) copy-start(bf16[88,2048]{1,0:T(8,128)(2,1)} %shared_up_ref.1) | copy-start | bytes 1081348
  17.7 10.2 %copy-start.6 = (f32[2048]{0:T(1024)S(1)}, f32[2048]{0:T(1024)}, u32[]{:S(2)}) copy-start(f32[2048]{0:T(1024)} %param.29) | copy-start | bytes 24580
  17.7 10.2 %copy-start.7 = (s32[16,6]{0,1:T(8,128)S(1)}, s32[16,6]{0,1:T(8,128)}, u32[]{:S(2)}) copy-start(s32[16,6]{0,1:T(8,128)} %param.36) | copy-start | bytes 1156
  17.7 10.2 %copy-start.8 = (f32[16,6]{0,1:T(8,128)S(1)}, f32[16,6]{0,1:T(8,128)}, u32[]{:S(2)}) copy-start(f32[16,6]{0,1:T(8,128)} %param.37) | copy-start | bytes 1156
  27.9 12.8 %copy-start.5 = (bf16[1408,128]{1,0:T(8,128)(2,1)S(1)}, bf16[1408,128]{1,0:T(8,128)(2,1)}, u32[]{:S(2)}) copy-start(bf16[1408,128]{1,0:T(8,128)(2,1)} %down_ref.1) | copy-start | bytes 1081348

commit v7 on v5

--- a/solution.py
+++ b/solution.py
@@ -161,6 +161,7 @@
 VMEM = pltpu.VMEM
 cuts = (0, 1, 4, 8)
 ahead = 2
+unit_step = 256
 
 
 def in_vmem():
@@ -425,22 +426,35 @@
     def against(matrix):
         return lax.dot_general(matrix, normed, contract_last, preferred_element_type=jnp.float32)
 
-    units = shared_gate_ref.shape[0]
-    spread = (
-        lax.broadcasted_iota(jnp.int32, (units, width), 0)
-        == lax.broadcasted_iota(jnp.int32, (units, width), 1)
-    ).astype(jnp.bfloat16)
-    contract_first = (((0,), (0,)), ((), ()))
-    halves = (against(gate_ref[...]), against(up_ref[...]))
-    shared_halves = (against(shared_gate_ref[...]), against(shared_up_ref[...]))
-    hidden = (silu_product(*halves) * share).astype(jnp.bfloat16)
-    result = lax.dot_general(
-        hidden, down_ref[...], contract_first, preferred_element_type=jnp.float32
-    ).astype(jnp.bfloat16)
-    shared_hidden = silu_product(*shared_halves).astype(jnp.bfloat16)
-    shared_rows = lax.dot_general(
-        shared_hidden, spread, contract_first, preferred_element_type=jnp.float32
-    ).astype(jnp.bfloat16)
+
+    tokens_eye = (
+        lax.broadcasted_iota(jnp.int32, (tokens, tokens), 0)
+        == lax.broadcasted_iota(jnp.int32, (tokens, tokens), 1)
+    )
+    share = jnp.sum(
+        jnp.where(tokens_eye, jnp.broadcast_to(share, (tokens, tokens)), 0.0),
+        axis=1,
+        keepdims=True,
+    )
+
+    def across(matrix):
+        return lax.dot_general(normed, matrix, contract_last, preferred_element_type=jnp.float32)
+
+    total = gate_ref.shape[0]
+    edges = list(range(0, total, unit_step)) + [total]
+    pairs = []
+    for low, high in zip(edges[:-1], edges[1:]):
+        pairs.append((against(gate_ref[low:high, :]), across(up_ref[low:high, :])))
+    shared_g = against(shared_gate_ref[...]).T
+    shared_u = across(shared_up_ref[...])
+
+    hidden = jnp.concatenate([(silu_product(g.T, u) * share).astype(jnp.bfloat16) for g, u in pairs], axis=1)
+    result = jnp.dot(hidden, down_ref[...], preferred_element_type=jnp.float32).astype(jnp.bfloat16)
+    shared_hidden = silu_product(shared_g, shared_u).astype(jnp.bfloat16)
+    units = shared_hidden.shape[1]
+    shared_rows = jnp.concatenate(
+        [shared_hidden, jnp.zeros((tokens, width - units), jnp.bfloat16)], axis=1
+    )
     for p in range(peers):
         out_ref[p, :tokens, :] = result[:, p * width : (p + 1) * width]
         out_ref[p, tokens:, :] = shared_rows

time: 41.4 us -> 41.2 us (level)
  no operation moved by 1% of the time
where the time goes in v7:
time: 41.2 us; the launch traced here: 41 us
  blocking collectives  34.1 us (83%)
  Pallas kernels  6.04 us (15%)
  between operations  0.81 us (2%)
    all_to_all x3, blocking collectives, exchange(): return lax.all_to_all(blocks, 'ep', split_axis=0, concat_axis=0, tiled=True)  34.1 us
    pallas_call x1, Pallas kernels, attend(): pl.pallas_call(attention_kernel, out_shape=VMEM((heads, size), bf16), in_...  2.86 us
    pallas_call x1, Pallas kernels, run_experts(): pl.pallas_call(expert_kernel, out_shape=VMEM((peers, 2 * tokens, width),...  2.12 us

profile of v7, /device:TPU:0, one launch (start us, length us, event | category | flops | bytes accessed | tf_op | source)
XLA Modules:
  0.0 41.0 jit_solution(14292084314723264987)
XLA Ops:
  0.7 2.9 %attention.1.own_ref = bf16[8,128]{1,0:T(8,128)(2,1)S(1)} custom-call(s32[1]{0:T(128)S(6)} %copy.20.lengths_ref, bf16[1,8,128]{2,1,0:T(8,128)(2,1)} %queries_hbm.1, bf16[1,2,128]{2,1,0:T(2,128)(2,1)} %fresh_hbm.1, bf16[1,2,128]{2,1,0:T(2,128)(2,1)} %value_new_hbm.1, f32[1,8]{1,0:T(1,128)} %forget_hbm.1, bf16[1,2,4096,128]{3,2,1,0:T(8,128)(2,1)} %keys_hbm.1, ...), custom_call_target="tpu_custom_call" | custom-call | tf_op jit(solution)/shard_map/attention/pallas_call | solution.py:334
  3.5 0.0 copy-start.6
  3.5 0.0 copy-start.8
  3.5 0.0 copy-start
  3.6 0.0 copy-start.1
  3.6 0.0 copy-start.2
  3.6 0.0 copy-start.3
  3.6 0.0 copy-start.4
  3.6 0.0 copy-start.7
  3.6 0.0 copy-start.9
  3.6 0.0 copy-start.10
  3.7 14.1 %all_to_all.15.rows_ref = bf16[16,8,128]{2,1,0:T(8,128)(2,1)S(1)} all-to-all(bf16[16,8,128]{2,1,0:T(8,128)(2,1)S(1)} %spread.1), channel_id=1, replica_groups=mesh['grp'=2,'ep'=16] {'ep'}, dimensions={0} | all-to-all | bytes 65536 | tf_op jit(solution)/shard_map/all_to_all | solution.py:525
  17.8 0.0 copy-done.6
  17.8 0.0 copy-done.8
  17.8 0.2 projection.1.stream_ref
  18.0 9.5 %all_to_all.16.blocks_ref = bf16[16,16,128]{2,1,0:T(8,128)(2,1)S(1)} all-to-all(bf16[16,16,128]{2,1,0:T(8,128)(2,1)S(1)} %projection.1.stream_ref), channel_id=1, replica_groups=mesh['grp'=2,'ep'=16] {'ep'}, dimensions={0} | all-to-all | bytes 131072 | tf_op jit(solution)/shard_map/all_to_all | solution.py:525
  27.5 0.0 copy-done
  27.5 0.0 copy-done.1
  27.5 0.0 copy-done.2
  27.5 0.0 copy-done.3
  27.5 0.0 copy-done.4
  27.5 0.0 copy-done.7
  27.5 0.0 copy-done.9
  27.5 0.0 copy-done.10
  27.6 0.0 copy-start.5
  27.6 2.1 %experts.1 = bf16[16,32,128]{2,1,0:T(8,128)(2,1)S(1)} custom-call(bf16[16,16,128]{2,1,0:T(8,128)(2,1)S(1)} %all_to_all.16.blocks_ref, f32[16,128]{1,0:T(8,128)S(1)} %bitcast.9, s32[6,16]{1,0:T(8,128)S(1)} %bitcast.10, f32[6,16]{1,0:T(8,128)S(1)} %bitcast.11, bf16[704,2048]{1,0:T(8,128)(2,1)S(1)} %bitcast.6, bf16[704,2048]{1,0:T(8,128)(2,1)S(1)} %bitcast.7, ...), custom_call_target="tpu_custom_call" | custom-call | tf_op jit(solution)/shard_map/experts/pallas_call | solution.py:476
  29.7 10.5 %all_to_all.17.received_ref = bf16[16,32,128]{2,1,0:T(8,128)(2,1)S(1)} all-to-all(bf16[16,32,128]{2,1,0:T(8,128)(2,1)S(1)} %experts.1), channel_id=1, replica_groups=mesh['grp'=2,'ep'=16] {'ep'}, dimensions={0} | all-to-all | bytes 262144 | tf_op jit(solution)/shard_map/all_to_all | solution.py:525
  40.2 0.0 copy-done.5
  40.2 0.8 %combine.1 = bf16[16,128]{1,0:T(8,128)(2,1)} custom-call(bf16[16,32,128]{2,1,0:T(8,128)(2,1)S(1)} %all_to_all.17.received_ref, bf16[16,16,128]{2,1,0:T(8,128)(2,1)S(1)} %projection.1.stream_ref, bf16[1408,128]{1,0:T(8,128)(2,1)S(1)} %copy-done.5), custom_call_target="tpu_custom_call" | custom-call | tf_op jit(solution)/shard_map/combine/pallas_call | solution.py:514
  (1 shorter events, 0.0 us)
Async XLA Ops:
  3.5 14.2 %copy-start.6 = (bf16[1024,128]{1,0:T(8,128)(2,1)S(1)}, bf16[1024,128]{1,0:T(8,128)(2,1)}, u32[]{:S(2)}) copy-start(bf16[1024,128]{1,0:T(8,128)(2,1)} %weight_ref.1) | copy-start | bytes 786436
  3.5 14.2 %copy-start.8 = (bf16[16,128]{1,0:T(8,128)(2,1)S(1)}, bf16[16,128]{1,0:T(8,128)(2,1)}, u32[]{:S(2)}) copy-start(bf16[16,128]{1,0:T(8,128)(2,1)} %residual_ref.1) | copy-start | bytes 12292
  3.5 23.9 %copy-start = (bf16[1,704,2048]{2,1,0:T(8,128)(2,1)S(1)}, bf16[1,704,2048]{2,1,0:T(8,128)(2,1)}, u32[]{:S(2)}) copy-start(bf16[1,704,2048]{2,1,0:T(8,128)(2,1)} %param.30) | copy-start | bytes 8650756
  3.6 23.9 %copy-start.1 = (bf16[1,704,2048]{2,1,0:T(8,128)(2,1)S(1)}, bf16[1,704,2048]{2,1,0:T(8,128)(2,1)}, u32[]{:S(2)}) copy-start(bf16[1,704,2048]{2,1,0:T(8,128)(2,1)} %param.31) | copy-start | bytes 8650756
  3.6 23.9 %copy-start.2 = (bf16[1,704,2048]{2,1,0:T(8,128)(2,1)S(1)}, bf16[1,704,2048]{2,1,0:T(8,128)(2,1)}, u32[]{:S(2)}) copy-start(bf16[1,704,2048]{2,1,0:T(8,128)(2,1)} %param.32) | copy-start | bytes 8650756
  3.6 23.9 %copy-start.3 = (bf16[88,2048]{1,0:T(8,128)(2,1)S(1)}, bf16[88,2048]{1,0:T(8,128)(2,1)}, u32[]{:S(2)}) copy-start(bf16[88,2048]{1,0:T(8,128)(2,1)} %shared_gate_ref.1) | copy-start | bytes 1081348
  3.6 23.9 %copy-start.4 = (bf16[88,2048]{1,0:T(8,128)(2,1)S(1)}, bf16[88,2048]{1,0:T(8,128)(2,1)}, u32[]{:S(2)}) copy-start(bf16[88,2048]{1,0:T(8,128)(2,1)} %shared_up_ref.1) | copy-start | bytes 1081348
  3.6 23.9 %copy-start.7 = (f32[2048]{0:T(1024)S(1)}, f32[2048]{0:T(1024)}, u32[]{:S(2)}) copy-start(f32[2048]{0:T(1024)} %param.29) | copy-start | bytes 24580
  3.6 23.9 %copy-start.9 = (s32[16,6]{0,1:T(8,128)S(1)}, s32[16,6]{0,1:T(8,128)}, u32[]{:S(2)}) copy-start(s32[16,6]{0,1:T(8,128)} %param.36) | copy-start | bytes 1156
  3.6 23.9 %copy-start.10 = (f32[16,6]{0,1:T(8,128)S(1)}, f32[16,6]{0,1:T(8,128)}, u32[]{:S(2)}) copy-start(f32[16,6]{0,1:T(8,128)} %param.37) | copy-start | bytes 1156
  27.6 12.6 %copy-start.5 = (bf16[1408,128]{1,0:T(8,128)(2,1)S(1)}, bf16[1408,128]{1,0:T(8,128)(2,1)}, u32[]{:S(2)}) copy-start(bf16[1408,128]{1,0:T(8,128)(2,1)} %down_ref.1) | copy-start | bytes 1081348

commit v8 on v7

--- a/solution.py
+++ b/solution.py
@@ -189,16 +189,13 @@
     keys_hbm,
     values_hbm,
     cumlog_hbm,
-    out_ref,
-    queries_ref,
-    fresh_ref,
-    value_new_ref,
-    forget_ref,
-    keys,
-    values,
-    scores,
-    sems,
+    *rest,
 ):
+    extra = (len(rest) - 9) // 2
+    side_hbm, (out_ref, *side_refs) = rest[:extra], rest[extra : 2 * extra + 1]
+    queries_ref, fresh_ref, value_new_ref, forget_ref, keys, values, scores, sems = rest[
+        2 * extra + 1 :
+    ]
     heads, size = queries_ref.shape
     key_heads, span, _ = keys.shape
     groups = heads // key_heads
@@ -233,7 +230,11 @@
 
     key_copies = copies(keys_hbm, keys, cuts, 0)
     value_copies = copies(values_hbm, values, cuts, len(cuts) - 1)
-    for copy in small_copies + key_copies + value_copies:
+    side_copies = [
+        pltpu.make_async_copy(source, target, sems.at[first + len(small_copies) + i])
+        for i, (source, target) in enumerate(zip(side_hbm, side_refs))
+    ]
+    for copy in small_copies + key_copies + value_copies + side_copies:
         copy.start()
 
     def side_by_side(ref, low, high):
@@ -317,8 +318,9 @@
         mine = mine + jnp.where(
             head_rows // groups == k, total[:, k * size : (k + 1) * size], 0.0
         )
-    attended = (mine / denominator).astype(jnp.bfloat16)
-    out_ref[...] = attended
+    out_ref[...] = (mine / denominator).astype(jnp.bfloat16)
+    for copy in side_copies:
+        copy.wait()
 
 
 def spread_kernel(own_ref, out_ref):
@@ -326,16 +328,26 @@
         out_ref[peer] = own_ref[...]
 
 
-def attend(queries, fresh_token_key, value_new, forget_logit, cache_keys, cache_values, cache_cumlog, lengths):
+def attend(
+    queries,
+    fresh_token_key,
+    value_new,
+    forget_logit,
+    cache_keys,
+    cache_values,
+    cache_cumlog,
+    lengths,
+    *side,
+):
     peers = lax.axis_size("ep")
     _, heads, size = queries.shape
     _, key_heads, span, _ = cache_keys.shape
     bf16 = jnp.bfloat16
-    own = pl.pallas_call(
+    own, *fetched = pl.pallas_call(
         attention_kernel,
-        out_shape=VMEM((heads, size), bf16),
-        in_specs=[pl.BlockSpec(memory_space=pltpu.SMEM)] + [in_hbm()] * 7,
-        out_specs=in_vmem(),
+        out_shape=[VMEM((heads, size), bf16)] + [VMEM(a.shape, a.dtype) for a in side],
+        in_specs=[pl.BlockSpec(memory_space=pltpu.SMEM)] + [in_hbm()] * (7 + len(side)),
+        out_specs=[in_vmem()] * (1 + len(side)),
         scratch_shapes=[
             VMEM((heads, size), bf16),
             VMEM((key_heads, size), bf16),
@@ -344,7 +356,7 @@
             VMEM((key_heads, span, size), bf16),
             VMEM((key_heads, span, size), bf16),
             VMEM((heads, span), jnp.float32),
-            pltpu.SemaphoreType.DMA((2 * len(cuts) + 3,)),
+            pltpu.SemaphoreType.DMA((2 * len(cuts) + 3 + len(side),)),
         ],
         compiler_params=params(12),
         name="attention",
@@ -358,9 +370,10 @@
             cache_keys,
             cache_values,
             cache_cumlog,
+            *side,
         ),
     )
-    return pl.pallas_call(
+    spread = pl.pallas_call(
         spread_kernel,
         out_shape=VMEM((peers, heads, size), bf16),
         in_specs=[in_vmem()],
@@ -371,6 +384,7 @@
         ),
         name="spread",
     )(own)
+    return spread, fetched
 
 
 def projection_kernel(rows_ref, weight_ref, residual_ref, out_ref):
@@ -460,17 +474,7 @@
         out_ref[p, tokens:, :] = shared_rows
 
 
-def run_experts(
-    blocks,
-    norm_gain,
-    routes,
-    route_scores,
-    expert_gate,
-    expert_up,
-    expert_down,
-    shared_gate,
-    shared_up,
-):
+def run_experts(blocks, fetched, expert_gate, expert_up, expert_down):
     peers, tokens, width = blocks.shape
     bf16 = jnp.bfloat16
     return pl.pallas_call(
@@ -482,12 +486,15 @@
         name="experts",
     )(
         blocks,
-        norm_gain.reshape(peers, width),
-        routes.T,
-        route_scores.T,
         *(
             pltpu.with_memory_space_constraint(a, VMEM)
-            for a in (expert_gate[0], expert_up[0], expert_down[0], shared_gate, shared_up)
+            for a in (
+                *fetched[:3],
+                expert_gate[0],
+                expert_up[0],
+                expert_down[0],
+                *fetched[3:],
+            )
         ),
     )
 
@@ -551,7 +558,7 @@
     _, key_heads, span, _ = cache_keys.shape
     tokens, width = residual.shape
     bf16 = jnp.bfloat16
-    spread = attend(
+    spread, fetched = attend(
         queries,
         fresh_token_key,
         value_new,
@@ -560,6 +567,11 @@
         cache_values,
         cache_cumlog,
         lengths,
+        norm_gain.reshape(peers, width),
+        routes.T,
+        route_scores.T,
+        shared_gate,
+        shared_up,
     )
     rows = exchange(spread)
     stream = pl.pallas_call(
@@ -571,17 +583,7 @@
         name="projection",
     )(rows, out_weight, residual)
     blocks = exchange(stream)
-    outgoing = run_experts(
-        blocks,
-        norm_gain,
-        routes,
-        route_scores,
-        expert_gate,
-        expert_up,
-        expert_down,
-        shared_gate,
-        shared_up,
-    )
+    outgoing = run_experts(blocks, fetched, expert_gate, expert_up, expert_down)
     received = exchange(outgoing)
     return combine(received, stream, shared_down)
 

time: 41.2 us -> 41.2 us (level)
  no operation moved by 1% of the time
where the time goes in v8:
time: 41.2 us; the launch traced here: 41 us
  blocking collectives  34.1 us (83%)
  Pallas kernels  6.1 us (15%)
  between operations  0.73 us (2%)
    all_to_all x3, blocking collectives, exchange(): return lax.all_to_all(blocks, 'ep', split_axis=0, concat_axis=0, tiled=True)  34.1 us
    pallas_call x1, Pallas kernels, attend(): pl.pallas_call(attention_kernel, out_shape=[VMEM((heads, size), bf16)] +...  2.92 us
    pallas_call x1, Pallas kernels, run_experts(): pl.pallas_call(expert_kernel, out_shape=VMEM((peers, 2 * tokens, width),...  2.12 us

profile of v8, /device:TPU:0, one launch (start us, length us, event | category | flops | bytes accessed | tf_op | source)
XLA Modules:
  0.0 41.0 jit_solution(3943025493029063445)
XLA Ops:
  0.7 2.9 %attention.1 = (bf16[8,128]{1,0:T(8,128)(2,1)S(1)}, f32[16,128]{1,0:T(8,128)S(1)}, s32[6,16]{1,0:T(8,128)S(1)}, f32[6,16]{1,0:T(8,128)S(1)}, bf16[88,2048]{1,0:T(8,128)(2,1)S(1)}, /*index=5*/bf16[88,2048]{1,0:T(8,128)(2,1)S(1)}) custom-call(s32[1]{0:T(128)S(6)} %copy.20.lengths_ref, bf16[1,8,128]{2,1,0:T(8,128)(2,1)} %queries_hbm.1, ...), custom_call_target="tpu_custom_call" | custom-call | tf_op jit(solution)/shard_map/attention/pallas_call | solution.py:346
  3.6 0.0 copy-start.4
  3.6 0.0 copy-start.5
  3.6 0.0 copy-start
  3.6 0.0 copy-start.1
  3.6 0.0 copy-start.2
  3.7 14.1 %all_to_all.15.rows_ref = bf16[16,8,128]{2,1,0:T(8,128)(2,1)S(1)} all-to-all(bf16[16,8,128]{2,1,0:T(8,128)(2,1)S(1)} %spread.1), channel_id=1, replica_groups=mesh['grp'=2,'ep'=16] {'ep'}, dimensions={0} | all-to-all | bytes 65536 | tf_op jit(solution)/shard_map/all_to_all | solution.py:532
  17.8 0.0 copy-done.4
  17.8 0.0 copy-done.5
  17.8 0.2 projection.1.stream_ref
  18.0 9.5 %all_to_all.16.blocks_ref = bf16[16,16,128]{2,1,0:T(8,128)(2,1)S(1)} all-to-all(bf16[16,16,128]{2,1,0:T(8,128)(2,1)S(1)} %projection.1.stream_ref), channel_id=1, replica_groups=mesh['grp'=2,'ep'=16] {'ep'}, dimensions={0} | all-to-all | bytes 131072 | tf_op jit(solution)/shard_map/all_to_all | solution.py:532
  27.5 0.0 copy-done
  27.5 0.0 copy-done.1
  27.5 0.0 copy-done.2
  27.5 0.0 copy-start.3
  27.5 2.1 %experts.1 = bf16[16,32,128]{2,1,0:T(8,128)(2,1)S(1)} custom-call(bf16[16,16,128]{2,1,0:T(8,128)(2,1)S(1)} %all_to_all.16.blocks_ref, f32[16,128]{1,0:T(8,128)S(1)} %get-tuple-element.12.gain_ref, s32[6,16]{1,0:T(8,128)S(1)} %get-tuple-element.13.routes_ref, f32[6,16]{1,0:T(8,128)S(1)} %get-tuple-element.14.scores_ref, bf16[704,2048]{1,0:T(8,128)(2,1)S(1)} %bitcast.6, ...), custom_call_target="tpu_custom_call" | custom-call | tf_op jit(solution)/shard_map/experts/pallas_call | solution.py:480
  29.6 10.5 %all_to_all.17.received_ref = bf16[16,32,128]{2,1,0:T(8,128)(2,1)S(1)} all-to-all(bf16[16,32,128]{2,1,0:T(8,128)(2,1)S(1)} %experts.1), channel_id=1, replica_groups=mesh['grp'=2,'ep'=16] {'ep'}, dimensions={0} | all-to-all | bytes 262144 | tf_op jit(solution)/shard_map/all_to_all | solution.py:532
  40.1 0.0 copy-done.3
  40.1 0.8 %combine.1 = bf16[16,128]{1,0:T(8,128)(2,1)} custom-call(bf16[16,32,128]{2,1,0:T(8,128)(2,1)S(1)} %all_to_all.17.received_ref, bf16[16,16,128]{2,1,0:T(8,128)(2,1)S(1)} %projection.1.stream_ref, bf16[1408,128]{1,0:T(8,128)(2,1)S(1)} %copy-done.3), custom_call_target="tpu_custom_call" | custom-call | tf_op jit(solution)/shard_map/combine/pallas_call | solution.py:521
  (1 shorter events, 0.0 us)
Async XLA Ops:
  3.6 14.2 %copy-start.4 = (bf16[1024,128]{1,0:T(8,128)(2,1)S(1)}, bf16[1024,128]{1,0:T(8,128)(2,1)}, u32[]{:S(2)}) copy-start(bf16[1024,128]{1,0:T(8,128)(2,1)} %weight_ref.1) | copy-start | bytes 786436
  3.6 14.2 %copy-start.5 = (bf16[16,128]{1,0:T(8,128)(2,1)S(1)}, bf16[16,128]{1,0:T(8,128)(2,1)}, u32[]{:S(2)}) copy-start(bf16[16,128]{1,0:T(8,128)(2,1)} %residual_ref.1) | copy-start | bytes 12292
  3.6 23.9 %copy-start = (bf16[1,704,2048]{2,1,0:T(8,128)(2,1)S(1)}, bf16[1,704,2048]{2,1,0:T(8,128)(2,1)}, u32[]{:S(2)}) copy-start(bf16[1,704,2048]{2,1,0:T(8,128)(2,1)} %param.30) | copy-start | bytes 8650756
  3.6 23.9 %copy-start.1 = (bf16[1,704,2048]{2,1,0:T(8,128)(2,1)S(1)}, bf16[1,704,2048]{2,1,0:T(8,128)(2,1)}, u32[]{:S(2)}) copy-start(bf16[1,704,2048]{2,1,0:T(8,128)(2,1)} %param.31) | copy-start | bytes 8650756
  3.6 23.9 %copy-start.2 = (bf16[1,704,2048]{2,1,0:T(8,128)(2,1)S(1)}, bf16[1,704,2048]{2,1,0:T(8,128)(2,1)}, u32[]{:S(2)}) copy-start(bf16[1,704,2048]{2,1,0:T(8,128)(2,1)} %param.32) | copy-start | bytes 8650756
  27.5 12.6 %copy-start.3 = (bf16[1408,128]{1,0:T(8,128)(2,1)S(1)}, bf16[1408,128]{1,0:T(8,128)(2,1)}, u32[]{:S(2)}) copy-start(bf16[1408,128]{1,0:T(8,128)(2,1)} %down_ref.1) | copy-start | bytes 1081348

commit v9 on v8

--- a/solution.py
+++ b/solution.py
@@ -474,7 +474,9 @@
         out_ref[p, tokens:, :] = shared_rows
 
 
-def run_experts(blocks, fetched, expert_gate, expert_up, expert_down):
+def run_experts(
+    blocks, fetched, expert_gate, expert_up, expert_down, shared_gate, shared_up
+):
     peers, tokens, width = blocks.shape
     bf16 = jnp.bfloat16
     return pl.pallas_call(
@@ -489,11 +491,12 @@
         *(
             pltpu.with_memory_space_constraint(a, VMEM)
             for a in (
-                *fetched[:3],
+                *fetched,
                 expert_gate[0],
                 expert_up[0],
                 expert_down[0],
-                *fetched[3:],
+                shared_gate,
+                shared_up,
             )
         ),
     )
@@ -570,8 +573,6 @@
         norm_gain.reshape(peers, width),
         routes.T,
         route_scores.T,
-        shared_gate,
-        shared_up,
     )
     rows = exchange(spread)
     stream = pl.pallas_call(
@@ -583,7 +584,9 @@
         name="projection",
     )(rows, out_weight, residual)
     blocks = exchange(stream)
-    outgoing = run_experts(blocks, fetched, expert_gate, expert_up, expert_down)
+    outgoing = run_experts(
+        blocks, fetched, expert_gate, expert_up, expert_down, shared_gate, shared_up
+    )
     received = exchange(outgoing)
     return combine(received, stream, shared_down)
 

time: 41.2 us -> 41.2 us (level)
  no operation moved by 1% of the time
where the time goes in v9:
time: 41.2 us; the launch traced here: 41 us
  blocking collectives  34.1 us (83%)
  Pallas kernels  6.08 us (15%)
  between operations  0.76 us (2%)
    all_to_all x3, blocking collectives, exchange(): return lax.all_to_all(blocks, 'ep', split_axis=0, concat_axis=0, tiled=True)  34.1 us
    pallas_call x1, Pallas kernels, attend(): pl.pallas_call(attention_kernel, out_shape=[VMEM((heads, size), bf16)] +...  2.89 us
    pallas_call x1, Pallas kernels, run_experts(): pl.pallas_call(expert_kernel, out_shape=VMEM((peers, 2 * tokens, width),...  2.13 us

profile of v9, /device:TPU:0, one launch (start us, length us, event | category | flops | bytes accessed | tf_op | source)
XLA Modules:
  0.0 41.0 jit_solution(7423987476895294533)
XLA Ops:
  0.7 2.9 %attention.1 = (bf16[8,128]{1,0:T(8,128)(2,1)S(1)}, f32[16,128]{1,0:T(8,128)S(1)}, s32[6,16]{1,0:T(8,128)S(1)}, f32[6,16]{1,0:T(8,128)S(1)}) custom-call(s32[1]{0:T(128)S(6)} %copy.20.lengths_ref, bf16[1,8,128]{2,1,0:T(8,128)(2,1)} %queries_hbm.1, bf16[1,2,128]{2,1,0:T(2,128)(2,1)} %fresh_hbm.1, bf16[1,2,128]{2,1,0:T(2,128)(2,1)} %value_new_hbm.1, ...), custom_call_target="tpu_custom_call" | custom-call | tf_op jit(solution)/shard_map/attention/pallas_call | solution.py:346
  3.6 0.0 copy-start.6
  3.6 0.0 copy-start.7
  3.6 0.0 copy-start
  3.6 0.0 copy-start.1
  3.6 0.0 copy-start.2
  3.6 0.0 copy-start.3
  3.6 0.0 copy-start.4
  3.7 14.1 %all_to_all.15.rows_ref = bf16[16,8,128]{2,1,0:T(8,128)(2,1)S(1)} all-to-all(bf16[16,8,128]{2,1,0:T(8,128)(2,1)S(1)} %spread.1), channel_id=1, replica_groups=mesh['grp'=2,'ep'=16] {'ep'}, dimensions={0} | all-to-all | bytes 65536 | tf_op jit(solution)/shard_map/all_to_all | solution.py:535
  17.8 0.0 copy-done.6
  17.8 0.0 copy-done.7
  17.8 0.2 projection.1.stream_ref
  18.0 9.5 %all_to_all.16.blocks_ref = bf16[16,16,128]{2,1,0:T(8,128)(2,1)S(1)} all-to-all(bf16[16,16,128]{2,1,0:T(8,128)(2,1)S(1)} %projection.1.stream_ref), channel_id=1, replica_groups=mesh['grp'=2,'ep'=16] {'ep'}, dimensions={0} | all-to-all | bytes 131072 | tf_op jit(solution)/shard_map/all_to_all | solution.py:535
  27.5 0.0 copy-done
  27.5 0.0 copy-done.1
  27.5 0.0 copy-done.2
  27.5 0.0 copy-done.3
  27.5 0.0 copy-done.4
  27.5 0.0 copy-start.5
  27.5 2.1 %experts.1 = bf16[16,32,128]{2,1,0:T(8,128)(2,1)S(1)} custom-call(bf16[16,16,128]{2,1,0:T(8,128)(2,1)S(1)} %all_to_all.16.blocks_ref, f32[16,128]{1,0:T(8,128)S(1)} %get-tuple-element.10.gain_ref, s32[6,16]{1,0:T(8,128)S(1)} %get-tuple-element.11.routes_ref, f32[6,16]{1,0:T(8,128)S(1)} %get-tuple-element.12.scores_ref, bf16[704,2048]{1,0:T(8,128)(2,1)S(1)} %bitcast.6, ...), custom_call_target="tpu_custom_call" | custom-call | tf_op jit(solution)/shard_map/experts/pallas_call | solution.py:482
  29.7 10.5 %all_to_all.17.received_ref = bf16[16,32,128]{2,1,0:T(8,128)(2,1)S(1)} all-to-all(bf16[16,32,128]{2,1,0:T(8,128)(2,1)S(1)} %experts.1), channel_id=1, replica_groups=mesh['grp'=2,'ep'=16] {'ep'}, dimensions={0} | all-to-all | bytes 262144 | tf_op jit(solution)/shard_map/all_to_all | solution.py:535
  40.2 0.0 copy-done.5
  40.2 0.8 %combine.1 = bf16[16,128]{1,0:T(8,128)(2,1)} custom-call(bf16[16,32,128]{2,1,0:T(8,128)(2,1)S(1)} %all_to_all.17.received_ref, bf16[16,16,128]{2,1,0:T(8,128)(2,1)S(1)} %projection.1.stream_ref, bf16[1408,128]{1,0:T(8,128)(2,1)S(1)} %copy-done.5), custom_call_target="tpu_custom_call" | custom-call | tf_op jit(solution)/shard_map/combine/pallas_call | solution.py:524
  (1 shorter events, 0.0 us)
Async XLA Ops:
  3.6 14.2 %copy-start.6 = (bf16[1024,128]{1,0:T(8,128)(2,1)S(1)}, bf16[1024,128]{1,0:T(8,128)(2,1)}, u32[]{:S(2)}) copy-start(bf16[1024,128]{1,0:T(8,128)(2,1)} %weight_ref.1) | copy-start | bytes 786436
  3.6 14.2 %copy-start.7 = (bf16[16,128]{1,0:T(8,128)(2,1)S(1)}, bf16[16,128]{1,0:T(8,128)(2,1)}, u32[]{:S(2)}) copy-start(bf16[16,128]{1,0:T(8,128)(2,1)} %residual_ref.1) | copy-start | bytes 12292
  3.6 23.9 %copy-start = (bf16[1,704,2048]{2,1,0:T(8,128)(2,1)S(1)}, bf16[1,704,2048]{2,1,0:T(8,128)(2,1)}, u32[]{:S(2)}) copy-start(bf16[1,704,2048]{2,1,0:T(8,128)(2,1)} %param.30) | copy-start | bytes 8650756
  3.6 23.9 %copy-start.1 = (bf16[1,704,2048]{2,1,0:T(8,128)(2,1)S(1)}, bf16[1,704,2048]{2,1,0:T(8,128)(2,1)}, u32[]{:S(2)}) copy-start(bf16[1,704,2048]{2,1,0:T(8,128)(2,1)} %param.31) | copy-start | bytes 8650756
  3.6 23.9 %copy-start.2 = (bf16[1,704,2048]{2,1,0:T(8,128)(2,1)S(1)}, bf16[1,704,2048]{2,1,0:T(8,128)(2,1)}, u32[]{:S(2)}) copy-start(bf16[1,704,2048]{2,1,0:T(8,128)(2,1)} %param.32) | copy-start | bytes 8650756
  3.6 23.9 %copy-start.3 = (bf16[88,2048]{1,0:T(8,128)(2,1)S(1)}, bf16[88,2048]{1,0:T(8,128)(2,1)}, u32[]{:S(2)}) copy-start(bf16[88,2048]{1,0:T(8,128)(2,1)} %shared_gate_ref.1) | copy-start | bytes 1081348
  3.6 23.9 %copy-start.4 = (bf16[88,2048]{1,0:T(8,128)(2,1)S(1)}, bf16[88,2048]{1,0:T(8,128)(2,1)}, u32[]{:S(2)}) copy-start(bf16[88,2048]{1,0:T(8,128)(2,1)} %shared_up_ref.1) | copy-start | bytes 1081348
  27.5 12.6 %copy-start.5 = (bf16[1408,128]{1,0:T(8,128)(2,1)S(1)}, bf16[1408,128]{1,0:T(8,128)(2,1)}, u32[]{:S(2)}) copy-start(bf16[1408,128]{1,0:T(8,128)(2,1)} %down_ref.1) | copy-start | bytes 1081348
